TPU v7x, 32 devices: a whole 2x2x4 slice. The times are simulated.
32 devices in a mesh: sp: 8 (over z, x), tp: 4 (over y, core).
Axes of the slice: x: 2, y: 2, z: 4, core: 2. Of those that a mesh axis runs over, the one named last changes fastest.
Arguments:
- tokens: bfloat16 [1024, 2048], P(('sp', 'tp')), may hold values from -6 to 6
- input_norm_gain: float32 [2048], replicated, may hold values from 0.1 to 1.9
- convolution_value_weight: bfloat16 [2048, 1024], P('sp', 'tp'), may hold values from -0.125 to 0.125
- convolution_gate_weight: bfloat16 [2048, 1024], P('sp', 'tp'), may hold values from -0.125 to 0.125
- depthwise_filter_taps: float32 [31, 1024], P(None, 'tp'), may hold values from -4 to 4
- channel_norm_gain: float32 [1024], P('tp'), may hold values from 0.1 to 1.9
- channel_norm_bias: float32 [1024], P('tp'), may hold values from -3 to 3
- query_projection_weight: bfloat16 [2048, 1024], P('sp', 'tp'), may hold values from -0.125 to 0.125
- forget_gate_weight: bfloat16 [2048, 1024], P('sp', 'tp'), may hold values from -0.125 to 0.125
- recurrence_value_weight: bfloat16 [2048, 1024], P('sp', 'tp'), may hold values from -0.125 to 0.125
- output_gate_weight: bfloat16 [2048, 1024], P('sp', 'tp'), may hold values from -0.125 to 0.125
- forget_floor_margin: float32 [1024], P('tp'), may hold values from 9.765625e-05 to 0.1
- decay_jump_terms: float32 [8, 1024], P('tp', 'sp'), may hold values from -0.7 to 0
- head_norm_gain: float32 [1024], P('tp'), may hold values from 0.1 to 1.9
- convolution_output_weight: bfloat16 [1024, 2048], P('tp', 'sp'), may hold values from -0.125 to 0.125
- recurrence_output_weight: bfloat16 [1024, 2048], P('tp', 'sp'), may hold values from -0.125 to 0.125
Outputs:
- mixed: bfloat16 [1024, 2048], P(('sp', 'tp'))
All inputs are finite; a program needn't handle non-finite values.
Results may differ from a plain program's by a relative error of at most 0.015.
Values may be sent and summed in bfloat16 or wider, within the bound.
A program may use at most 64 MiB of HBM per device.

v0:
```python
import jax
import jax.numpy as jnp
from jax import lax
from jax.sharding import PartitionSpec as P

CONV_CH = 1024
HG_DK = 128
HG_DV = 128
HG_BLOCK = 64


norm_eps = 1e-06
layer_eps = 1e-05
highest_precision = lax.Precision.HIGHEST


def passed_along(value, axis, steps):
    count = lax.axis_size(axis)
    initial, last = (max(0, -steps), min(count, count - steps))
    return lax.ppermute(value, axis, [(source, source + steps) for source in range(initial, last)])


def prefix(x, axis, combine, identity):
    size, mine = (lax.axis_size(axis), lax.axis_index(axis))
    everything = jax.tree.map(
        lambda part, kind: lax.all_gather(part.astype(kind), axis), x, (jnp.bfloat16, jnp.bfloat16)
    )
    start = jax.tree.map(
        lambda part, zero: jnp.broadcast_to(jnp.asarray(zero, part.dtype), part.shape), x, identity
    )

    def lap(k, before):
        reached = k < mine
        new = combine(
            before, jax.tree.map(lambda part, own: part[k].astype(own.dtype), everything, x)
        )
        return jax.tree.map(lambda a, b: jnp.where(reached, a, b), new, before)

    return lax.fori_loop(0, size, lap, start)


def convolve(gated, kernel):
    return lax.conv_general_dilated(
        gated[None],
        kernel[:, None, :],
        (1,),
        "VALID",
        dimension_numbers=("NWC", "WIO", "NWC"),
        feature_group_count=gated.shape[1],
        precision=highest_precision,
    )[0]


def channel_norm(values, first_sum, second_sum, gain, bias):
    mean_value = first_sum[:, None] / CONV_CH
    variance = second_sum[:, None] / CONV_CH - mean_value * mean_value
    shifted = (values - mean_value) * lax.rsqrt(variance + layer_eps) * gain + bias
    return jax.nn.silu(shifted).astype(jnp.bfloat16)


def gate_factors(query_projected, forget_projected, forget_floor_margin, decay_jump_rows):
    row_total_count = query_projected.shape[0]
    head_total_count = decay_jump_rows.shape[1]
    query_rows = jax.nn.silu(query_projected.astype(jnp.float32))
    log_forget_gate = jnp.logaddexp(
        jnp.log1p(-forget_floor_margin),
        jnp.log(forget_floor_margin) + jax.nn.log_sigmoid(forget_projected.astype(jnp.float32)),
    )
    key_gate_values = -jnp.expm1(log_forget_gate)
    log_decay_running = (
        log_forget_gate.reshape(row_total_count, head_total_count, -1) + decay_jump_rows[:, :, None]
    )
    return (
        query_rows.reshape(row_total_count, head_total_count, -1),
        key_gate_values.reshape(row_total_count, head_total_count, -1),
        log_decay_running,
    )


def finish(recurrent, gain, outgate_proj):
    row_total_count = recurrent.shape[0]
    scaled = recurrent * lax.rsqrt(
        jnp.mean(recurrent * recurrent, axis=2, keepdims=True) + norm_eps
    )
    gated_out = (
        scaled.reshape(row_total_count, -1) * gain * jax.nn.silu(outgate_proj.astype(jnp.float32))
    )
    return gated_out.astype(jnp.bfloat16)


def combine_states(first_part, second_part):
    return (
        first_part[0] + second_part[0],
        jnp.exp(second_part[0])[:, :, None] * first_part[1] + second_part[1],
    )


def carry_step(recurrence_state, block_parts):
    decay_end, contribution = block_parts
    return (jnp.exp(decay_end)[:, :, None] * recurrence_state + contribution, recurrence_state)


def per_device(
    tokens,
    input_norm_gain,
    convolution_value_weight,
    convolution_gate_weight,
    depthwise_filter_taps,
    channel_norm_gain,
    channel_norm_bias,
    query_projection_weight,
    forget_gate_weight,
    recurrence_value_weight,
    output_gate_weight,
    forget_floor_margin,
    decay_jump_terms,
    head_norm_gain,
    convolution_output_weight,
    recurrence_output_weight,
):
    features = tokens.astype(jnp.float32)
    normed = (
        features
        * lax.rsqrt(jnp.mean(features * features, axis=1, keepdims=True) + norm_eps)
        * input_norm_gain
    ).astype(jnp.bfloat16)
    gathered = (
        lax.all_gather(convolution_value_weight, "sp", axis=0, tiled=True),
        lax.all_gather(convolution_gate_weight, "sp", axis=0, tiled=True),
        lax.all_gather(query_projection_weight, "sp", axis=0, tiled=True),
        lax.all_gather(forget_gate_weight, "sp", axis=0, tiled=True),
        lax.all_gather(recurrence_value_weight, "sp", axis=0, tiled=True),
        lax.all_gather(output_gate_weight, "sp", axis=0, tiled=True),
        lax.all_gather(convolution_output_weight, "sp", axis=1, tiled=True),
        lax.all_gather(recurrence_output_weight, "sp", axis=1, tiled=True),
    )
    projection_weights = gathered[:6]
    conv_columns = gathered[6]
    rec_columns = gathered[7]

    def project(row_piece):
        return jnp.concatenate(
            [
                jnp.dot(row_piece, weight, preferred_element_type=jnp.float32).astype(jnp.bfloat16)
                for weight in projection_weights
            ],
            axis=1,
        )

    projected = project(lax.all_gather(normed, "tp", axis=0, tiled=True))
    offsets = []
    position = 0
    for weight in projection_weights[:-1]:
        position = position + weight.shape[1]
        offsets.append(position)
    value_proj, gate_proj, query_projected, forget_projected, input_proj, outgate_proj = jnp.split(
        projected, offsets, axis=1
    )
    row_total_count = value_proj.shape[0]
    rim_rows = depthwise_filter_taps.shape[0] - 1
    tail_value, tail_gate = passed_along(
        (value_proj[row_total_count - rim_rows :], gate_proj[row_total_count - rim_rows :]), "sp", 1
    )
    value_ext = jnp.concatenate([tail_value, value_proj], axis=0)
    gate_ext = jnp.concatenate([tail_gate, gate_proj], axis=0)
    gated = value_ext.astype(jnp.float32) * jax.nn.sigmoid(gate_ext.astype(jnp.float32))
    convolved = convolve(gated, depthwise_filter_taps).astype(jnp.bfloat16)
    device_heads = decay_jump_terms.shape[0]
    query_rows, key_gate_values, log_decay_running = gate_factors(
        query_projected, forget_projected, forget_floor_margin, decay_jump_terms.T
    )
    input_rows = input_proj.astype(jnp.float32).reshape(row_total_count, device_heads, -1)
    block_count = row_total_count // HG_BLOCK

    def to_blocks(array):
        return array.reshape(block_count, HG_BLOCK, device_heads, -1).transpose(0, 2, 1, 3)

    block_queries = to_blocks(query_rows)
    block_keys = to_blocks(key_gate_values)
    block_inputs = to_blocks(input_rows)
    cumulative = jnp.cumsum(to_blocks(log_decay_running), axis=2)
    final_decay = cumulative[:, :, -1, :]
    query_rows_scaled = block_queries * jnp.exp(cumulative)
    scaled_keys = block_keys * jnp.exp(-cumulative)
    final_keys = block_keys * jnp.exp(final_decay[:, :, None, :] - cumulative)
    attention_scores = jnp.einsum(
        "nhtk,nhsk->nhts", query_rows_scaled, scaled_keys, precision=highest_precision
    )
    causal = jnp.arange(HG_BLOCK)[:, None] >= jnp.arange(HG_BLOCK)[None, :]
    attention_scores = jnp.where(causal[None, None], attention_scores, 0.0)
    inner = jnp.einsum(
        "nhts,nhsv->nhtv", attention_scores, block_inputs, precision=highest_precision
    )
    contributions = jnp.einsum(
        "nhsk,nhsv->nhkv", final_keys, block_inputs, precision=highest_precision
    )
    initial = jnp.zeros((device_heads, HG_DK, HG_DV), jnp.float32)
    local_state, block_starts = lax.scan(carry_step, initial, (final_decay, contributions))
    device_decay = jnp.sum(final_decay, axis=0)
    before_blocks = jnp.cumsum(final_decay, axis=0) - final_decay
    incoming = prefix(
        (device_decay, local_state),
        "sp",
        combine_states,
        (jnp.zeros_like(device_decay), jnp.zeros_like(local_state)),
    )
    starts = block_starts + jnp.exp(before_blocks)[:, :, :, None] * incoming[1][None]
    recurrent = inner + jnp.einsum(
        "nhtk,nhkv->nhtv", query_rows_scaled, starts, precision=highest_precision
    )
    recurrent = recurrent.transpose(0, 2, 1, 3).reshape(row_total_count, device_heads, -1)
    rec_out = finish(recurrent, head_norm_gain, outgate_proj)
    values = convolved.astype(jnp.float32)
    totals = lax.psum((jnp.sum(values, axis=1), jnp.sum(values * values, axis=1)), "tp")
    conv_out = channel_norm(values, totals[0], totals[1], channel_norm_gain, channel_norm_bias)
    conv_part = lax.slice_in_dim(
        conv_out, 0, row_total_count // lax.axis_size("tp") * lax.axis_size("tp"), axis=0
    )
    return lax.psum_scatter(
        (
            jnp.dot(conv_part, conv_columns, preferred_element_type=jnp.float32)
            + jnp.dot(rec_out, rec_columns, preferred_element_type=jnp.float32)
        ).astype(jnp.bfloat16),
        "tp",
        scatter_dimension=0,
        tiled=True,
    )


def solution(mesh):
    in_specs = (
        P(("sp", "tp"), None),
        P(),
        P("sp", "tp"),
        P("sp", "tp"),
        P(None, "tp"),
        P("tp"),
        P("tp"),
        P("sp", "tp"),
        P("sp", "tp"),
        P("sp", "tp"),
        P("sp", "tp"),
        P("tp"),
        P("tp", "sp"),
        P("tp"),
        P("tp", "sp"),
        P("tp", "sp"),
    )
    out_specs = P(("sp", "tp"), None)
    return jax.shard_map(
        per_device, mesh=mesh, in_specs=in_specs, out_specs=out_specs, check_vma=False
    )
```

profile of v0, /device:TPU:0, one launch (start us, length us, event | category | flops | bytes accessed | tf_op | source)
XLA Modules:
  0.0 371.7 jit_solution(17329059093912126885)
XLA Ops:
  6.5 0.7 all-gather.20.cloned.1.call-update
  7.3 0.7 all-gather.22.cloned.1.call-update
  8.1 0.7 all-gather.18.cloned.1.call-update
  8.8 0.5 all-gather.12.cloned.1.call-update
  9.4 0.5 all-gather.14.cloned.1.call-update
  10.0 0.5 all-gather.16.cloned.1.call-update
  10.5 0.7 all-gather.24.cloned.1.call-update
  11.3 0.7 all-gather.26.cloned.1.call-update
  12.1 0.1 fusion.9
  12.3 0.5 copy-done.2
  12.8 0.1 fusion.11
  12.9 8.7 %all_gather.37 = bf16[128,2048]{1,0:T(8,128)(2,1)S(1)} all-gather(bf16[32,2048]{1,0:T(8,128)(2,1)S(1)} %fusion.11), channel_id=1, replica_groups=mesh['sp'=8,'tp'=4] {'tp'}, dimensions={0}, use_global_device_ids=true | all-gather | bytes 655360 | tf_op jit(solution)/shard_map/all_gather | solution.py:150
  21.6 0.7 copy-done.7
  22.3 0.1 add.159
  22.4 30.1 %all-gather.20.cloned.1.call-done = bf16[2048,256]{1,0:T(8,128)(2,1)} async-done(((bf16[256,256]{1,0:T(8,128)(2,1)}), bf16[2048,256]{1,0:T(8,128)(2,1)}) %all-gather.20.cloned.1.call-update) | async-done | bytes 1048592 | tf_op jit(solution)/shard_map/all_gather | solution.py:131
  52.5 1.7 exponential-minus-one_negate_fusion
  54.2 0.1 reshape.180
  54.3 0.1 fusion.25
  54.4 0.1 reduce_window_sum.22
  54.6 0.1 reshape_reshape.10
  54.6 39.0 %all-gather.22.cloned.1.call-done = bf16[2048,256]{1,0:T(8,128)(2,1)} async-done(((bf16[256,256]{1,0:T(8,128)(2,1)}), bf16[2048,256]{1,0:T(8,128)(2,1)}) %all-gather.22.cloned.1.call-update) | async-done | bytes 1048592 | tf_op jit(solution)/shard_map/all_gather | solution.py:132
  93.6 1.5 convolution_convert_fusion.2
  95.2 0.4 fusion.24
  95.6 0.4 while.27
  95.7 0.1 bitcast_add_fusion.2
  95.8 0.1 bitcast_add_fusion.2
  96.0 32.5 %all-gather.1 = bf16[16,128,128]{2,1,0:T(8,128)(2,1)S(1)} all-gather(bf16[2,128,128]{2,1,0:T(8,128)(2,1)S(1)} %convert_element_type.128), channel_id=3, replica_groups=mesh['sp'=8,'tp'=4] {'sp'}, dimensions={0}, use_global_device_ids=true | all-gather | bytes 589824 | tf_op jit(solution)/shard_map/all_gather | solution.py:26
  128.5 17.8 %all-gather.2 = bf16[8,2,128]{2,1,0:T(2,128)(2,1)S(1)} all-gather(bf16[1,2,128]{2,1,0:T(2,128)(2,1)S(1)} %bitcast.113), channel_id=2, replica_groups=mesh['sp'=8,'tp'=4] {'sp'}, dimensions={0}, use_global_device_ids=true | all-gather | bytes 4608 | tf_op jit(solution)/shard_map/all_gather | solution.py:26
  146.3 1.4 while.28
  146.3 0.1 fusion.69
  146.5 0.1 fusion.69
  146.7 0.1 fusion.69
  146.9 0.1 fusion.69
  147.0 0.1 fusion.69
  147.2 0.1 fusion.69
  147.4 0.1 fusion.69
  147.6 0.1 fusion.69
  147.7 1.6 divide_multiply_fusion.1
  149.3 0.1 reshape_reshape.9
  149.4 28.2 %all-gather.12.cloned.1.call-done = bf16[2048,256]{1,0:T(8,128)(2,1)} async-done(((bf16[256,256]{1,0:T(8,128)(2,1)}), bf16[2048,256]{1,0:T(8,128)(2,1)}) %all-gather.12.cloned.1.call-update) | async-done | bytes 1048592 | tf_op jit(solution)/shard_map/all_gather | solution.py:128
  177.6 1.5 convolution_convert_fusion.6
  179.1 2.5 collective-permute-start
  181.6 36.9 %all-gather.14.cloned.1.call-done = bf16[2048,256]{1,0:T(8,128)(2,1)} async-done(((bf16[256,256]{1,0:T(8,128)(2,1)}), bf16[2048,256]{1,0:T(8,128)(2,1)}) %all-gather.14.cloned.1.call-update) | async-done | bytes 1048592 | tf_op jit(solution)/shard_map/all_gather | solution.py:129
  218.6 1.5 convolution_convert_fusion.5
  220.1 2.5 collective-permute-start.1
  222.6 0.4 convolution_select_fusion
  223.0 0.2 fusion.36
  223.2 0.5 multiply_reduce_fusion
  223.8 0.1 copy.43
  223.9 0.1 copy.40
  224.0 0.1 collective-permute-done.1
  224.1 0.1 divide_multiply_fusion
  224.2 2.2 fusion.51
  226.3 0.1 fusion.23
  226.4 5.7 %all-reduce = (f32[128]{0:T(128)S(1)}, f32[128]{0:T(128)S(1)}) all-reduce(f32[128]{0:T(128)S(1)} %fusion.23, f32[128]{0:T(128)S(1)} %get-tuple-element.194), channel_id=1, replica_groups=mesh['sp'=8,'tp'=4] {'tp'}, use_global_device_ids=true, to_apply=%region_4.5 | all-reduce | flops 256 | bytes 2048 | tf_op jit(solution)/shard_map/psum | solution.py:214
  232.1 26.5 %all-gather.16.cloned.1.call-done = bf16[256,2048]{1,0:T(8,128)(2,1)} async-done(((bf16[256,256]{1,0:T(8,128)(2,1)}), bf16[256,2048]{1,0:T(8,128)(2,1)}) %all-gather.16.cloned.1.call-update) | async-done | bytes 1048592 | tf_op jit(solution)/shard_map/all_gather | solution.py:134
  258.7 0.7 copy-done.3
  259.3 1.6 fusion.34
  261.0 39.2 %all-gather.24.cloned.1.call-done = bf16[2048,256]{1,0:T(8,128)(2,1)} async-done(((bf16[256,256]{1,0:T(8,128)(2,1)}), bf16[2048,256]{1,0:T(8,128)(2,1)}) %all-gather.24.cloned.1.call-update) | async-done | bytes 1048592 | tf_op jit(solution)/shard_map/all_gather | solution.py:133
  300.1 40.2 %all-gather.26.cloned.1.call-done = bf16[256,2048]{1,0:T(8,128)(2,1)} async-done(((bf16[256,256]{1,0:T(8,128)(2,1)}), bf16[256,2048]{1,0:T(8,128)(2,1)}) %all-gather.26.cloned.1.call-update) | async-done | bytes 1048592 | tf_op jit(solution)/shard_map/all_gather | solution.py:135
  340.3 0.2 mul.161
  340.5 0.7 copy-done.5
  341.2 3.1 fusion.1
  344.3 20.9 %reduce-scatter.2.cloned.1.call-done = bf16[32,2048]{1,0:T(8,128)(2,1)} async-done(((bf16[128,2048]{1,0:T(8,128)(2,1)}), bf16[32,2048]{1,0:T(8,128)(2,1)}) %reduce-scatter.2.cloned.1.call-update) | async-done | bytes 131088 | tf_op jit(solution)/shard_map/reduce_scatter | solution.py:219
  (51 shorter events, 0.6 us)
Async XLA Ops:
  6.5 217.6 %copy-start = (f32[31,256]{1,0:T(8,128)S(1)}, f32[31,256]{1,0:T(8,128)}, u32[]{:S(2)}) copy-start(f32[31,256]{1,0:T(8,128)} %param.24) | copy-start | bytes 95236
  6.5 46.0 %all-gather.20.cloned.1.call-start = ((), (), s32[]{:S(2)}) async-start(), calls=%async_computation.5 | async-start | bytes 1179648 | tf_op jit(solution)/shard_map/all_gather | solution.py:131
  7.3 86.4 %all-gather.22.cloned.1.call-start = ((), (), s32[]{:S(2)}) async-start(), calls=%async_computation.6 | async-start | bytes 1179648 | tf_op jit(solution)/shard_map/all_gather | solution.py:132
  8.0 139.7 %all-gather.18.cloned.1.call-start = ((), (), s32[]{:S(2)}) async-start(), calls=%async_computation.4 | async-start | bytes 1179648 | tf_op jit(solution)/shard_map/all_gather | solution.py:130
  8.7 168.8 %all-gather.12.cloned.1.call-start = ((), (), s32[]{:S(2)}) async-start(), calls=%async_computation.1 | async-start | bytes 1179648 | tf_op jit(solution)/shard_map/all_gather | solution.py:128
  9.3 209.3 %all-gather.14.cloned.1.call-start = ((), (), s32[]{:S(2)}) async-start(), calls=%async_computation.2 | async-start | bytes 1179648 | tf_op jit(solution)/shard_map/all_gather | solution.py:129
  9.9 248.8 %all-gather.16.cloned.1.call-start = ((), (), s32[]{:S(2)}) async-start(), calls=%async_computation.3 | async-start | bytes 1179648 | tf_op jit(solution)/shard_map/all_gather | solution.py:134
  10.5 1.6 copy-start.1
  10.5 289.6 %all-gather.24.cloned.1.call-start = ((), (), s32[]{:S(2)}) async-start(), calls=%async_computation.7 | async-start | bytes 1179648 | tf_op jit(solution)/shard_map/all_gather | solution.py:133
  11.2 329.1 %all-gather.26.cloned.1.call-start = ((), (), s32[]{:S(2)}) async-start(), calls=%async_computation.8 | async-start | bytes 1179648 | tf_op jit(solution)/shard_map/all_gather | solution.py:135
  12.0 353.2 %reduce-scatter.2.cloned.1.call-start = ((), (), s32[]{:S(2)}) async-start(), calls=%async_computation.9 | async-start | bytes 655360 | tf_op jit(solution)/shard_map/reduce_scatter | solution.py:219
  12.1 0.7 copy-start.2
  12.9 8.7 %copy-start.6 = (f32[256]{0:T(256)S(1)}, f32[256]{0:T(256)}, u32[]{:S(2)}) copy-start(f32[256]{0:T(256)} %param.31) | copy-start | bytes 3076
  21.6 0.7 copy-start.7
  179.1 44.9 %collective-permute-start = (bf16[30,256]{1,0:T(8,128)(2,1)S(1)}, bf16[30,256]{1,0:T(8,128)(2,1)S(1)}, u32[]{:S(2)}, u32[]{:S(2)}) collective-permute-start(bf16[30,256]{1,0:T(8,128)(2,1)S(1)} %slice.12), channel_id=1, source_target_pairs={{0,4},{4,8},{8,12},{12,16},{16,20},{20,24},{24,28},{1,5},{5,9},{9,... | collective-permute-start | bytes 46088 | tf_op jit(solution)/shard_map/ppermute | solution.py:20
  220.1 3.9 %collective-permute-start.1 = (bf16[30,256]{1,0:T(8,128)(2,1)S(1)}, bf16[30,256]{1,0:T(8,128)(2,1)S(1)}, u32[]{:S(2)}, u32[]{:S(2)}) collective-permute-start(bf16[30,256]{1,0:T(8,128)(2,1)S(1)} %slice.13), channel_id=1, source_target_pairs={{0,4},{4,8},{8,12},{12,16},{16,20},{20,24},{24,28},{1,5},{5,9},{9,... | collective-permute-start | bytes 46088 | tf_op jit(solution)/shard_map/ppermute | solution.py:20
  224.1 34.5 %copy-start.4 = (f32[256]{0:T(256)S(1)}, f32[256]{0:T(256)}, u32[]{:S(2)}) copy-start(f32[256]{0:T(256)} %param.25) | copy-start | bytes 3076
  258.7 0.7 copy-start.3
  340.5 0.7 copy-start.5
Sparse Core Ops, SparseCore 0:
  9.5 42.9 all-gather.19
  54.6 38.9 all-gather.21
  95.8 40.5 all-gather.17
  138.4 39.1 all-gather.11
  179.6 38.9 all-gather.13
  220.5 38.1 all-gather.15
  260.8 39.2 all-gather.23
  302.2 38.0 all-gather.25
  344.5 20.6 reduce-scatter.1
where the time goes:
time: 372 us
  waiting for transfers between devices  266 us (72%)
  blocking collectives  64.7 us (17%)
  matrix products  16.3 us (4%)
  between operations  13.5 us (4%)
  starting transfers between devices  5.28 us (1%)
    all_gather x2, blocking collectives, prefix(): lax.all_gather(part.astype(kind), axis)  50.3 us
    all_gather x1, waiting for transfers between devices, per_device(): lax.all_gather(recurrence_output_weight, 'sp', axis=1, tiled=True)  40.2 us
    all_gather x1, waiting for transfers between devices, per_device(): lax.all_gather(output_gate_weight, 'sp', axis=0, tiled=True)  39.2 us
    all_gather x1, waiting for transfers between devices, per_device(): lax.all_gather(recurrence_value_weight, 'sp', axis=0, tiled=True)  39 us
    all_gather x1, waiting for transfers between devices, per_device(): lax.all_gather(convolution_gate_weight, 'sp', axis=0, tiled=True)  36.9 us
    all_gather x1, waiting for transfers between devices, per_device(): lax.all_gather(forget_gate_weight, 'sp', axis=0, tiled=True)  30.1 us
    all_gather x1, waiting for transfers between devices, per_device(): lax.all_gather(convolution_value_weight, 'sp', axis=0, tiled=True)  28.2 us
    all_gather x1, waiting for transfers between devices, per_device(): lax.all_gather(convolution_output_weight, 'sp', axis=1, tiled=True)  26.5 us
  transfers between devices with their start and end apart: 11, of which 8 were waited for; matrix products, arithmetic and copies ran while one was open for 4% of the time, Pallas kernels for 0%

commit v1 on v0

--- a/solution.py
+++ b/solution.py
@@ -1,6 +1,10 @@
+import functools
+
 import jax
 import jax.numpy as jnp
 from jax import lax
+from jax.experimental import pallas as pl
+from jax.experimental.pallas import tpu as pltpu
 from jax.sharding import PartitionSpec as P
 
 CONV_CH = 1024
@@ -227,6 +231,438 @@
     )
 
 
+MESH = pl.DeviceIdType.MESH
+STRIDE = 2
+NT = (((1,), (1,)), ((), ()))
+TN = (((0,), (0,)), ((), ()))
+
+
+def at(sp, tp):
+    return {"sp": sp, "tp": tp}
+
+
+def greet(peers):
+    barrier = pltpu.get_barrier_semaphore()
+    for peer in peers:
+        pl.semaphore_signal(barrier, inc=1, device_id=peer, device_id_type=MESH)
+    pl.semaphore_wait(barrier, len(peers))
+
+
+def remote(src, dst, send, recv, peer):
+    return pltpu.make_async_remote_copy(
+        src_ref=src, dst_ref=dst, send_sem=send, recv_sem=recv, device_id=peer, device_id_type=MESH
+    )
+
+
+def project_kernel(
+    sizes, x_ref, w_ref, j_ref, p_ref, qf_ref, jump_ref, held, weights, *sems
+):
+    n_sp, n_tp, rows, depth, chans, members = sizes
+    (send_z, send_x, send_y, send_c, lane, sib, send_w, recv_w, send_j, recv_j, send_q, recv_q) = sems
+    s, t = lax.axis_index("sp"), lax.axis_index("tp")
+    n_z = n_sp // STRIDE
+    z, x = s // STRIDE, s % STRIDE
+    y, c = t // 2, t % 2
+    x_peer = at(z * STRIDE + (1 - x), t)
+    y_peer = at(s, (1 - y) * 2 + c)
+    c_peer = at(s, y * 2 + (1 - c))
+
+    def sp_peer(k):
+        return lax.rem(s + k, n_sp)
+
+    def slot(dy, dx, dz, core):
+        from_z = lax.rem(z - dz + n_z, n_z)
+        from_x = (1 - x) if dx else x
+        from_y = (1 - y) if dy else y
+        shard = (from_z * STRIDE + from_x) * n_tp + from_y * 2 + core
+        return pl.ds(pl.multiple_of(shard * rows, rows), rows)
+
+    def number(dy, dx, dz):
+        return (dy * STRIDE + dx) * n_z + dz
+
+    greet([at(sp_peer(k), t) for k in range(1, n_sp)] + [y_peer, c_peer])
+    pending = []
+
+    def launch(copy):
+        copy.start()
+        pending.append(copy)
+
+    own = slot(0, 0, 0, c)
+
+    def pass_on(dy, dx, dz, src):
+        here = slot(dy, dx, dz, c)
+        at_number = number(dy, dx, dz)
+        if not dy:
+            if not dx:
+                launch(remote(src, held.at[here], send_x.at[dz], lane.at[number(0, 1, dz)], x_peer))
+            launch(remote(src, held.at[here], send_y.at[at_number], lane.at[number(1, dx, dz)], y_peer))
+        launch(remote(src, held.at[here], send_c.at[at_number], sib.at[at_number], c_peer))
+
+    for k in range(1, n_z):
+        peer = at(lax.rem(z + k, n_z) * STRIDE + x, t)
+        launch(remote(x_ref, held.at[own], send_z.at[k], lane.at[k], peer))
+    pass_on(0, 0, 0, x_ref)
+    my_columns = pl.ds(pl.multiple_of(s * depth, depth), depth)
+    for k in range(1, n_sp):
+        launch(remote(j_ref, jump_ref.at[s], send_j.at[k], recv_j.at[k], at(sp_peer(k), t)))
+    for k in range(1, n_sp):
+        launch(
+            remote(w_ref.at[sp_peer(k)], weights.at[:, my_columns], send_w.at[k], recv_w.at[k], at(sp_peer(k), t))
+        )
+    held[own, :] = x_ref[...]
+    jump_ref[s] = j_ref[...]
+    weights[:, my_columns] = w_ref[s]
+
+    def arrived(dy, dx, dz):
+        here = held.at[slot(dy, dx, dz, c)]
+        remote(here, here, send_c.at[0], lane.at[number(dy, dx, dz)], c_peer).wait_recv()
+        pass_on(dy, dx, dz, here)
+
+    for dz in range(1, n_z):
+        arrived(0, 0, dz)
+    for dz in range(n_z):
+        arrived(0, 1, dz)
+    for dx in range(STRIDE):
+        for dz in range(n_z):
+            arrived(1, dx, dz)
+    for k in range(1, n_sp):
+        source = lax.rem(s - k + n_sp, n_sp)
+        there = weights.at[:, pl.ds(pl.multiple_of(source * depth, depth), depth)]
+        remote(there, there, send_w.at[k], recv_w.at[k], c_peer).wait_recv()
+        remote(j_ref, jump_ref.at[source], send_j.at[k], recv_j.at[k], c_peer).wait_recv()
+    for dy in range(2):
+        for dx in range(STRIDE):
+            for dz in range(n_z):
+                here = held.at[slot(dy, dx, dz, 1 - c)]
+                remote(here, here, send_c.at[0], sib.at[number(dy, dx, dz)], c_peer).wait_recv()
+
+    member = lax.rem(s, members)
+    first = s - member
+    total = held.shape[0]
+    step = min(256, total)
+    for start in range(0, total, step):
+        piece = lax.dot_general(
+            held[start : start + step, :], weights[...], NT, preferred_element_type=jnp.float32
+        ).T.astype(jnp.bfloat16)
+        p_ref[:, start : start + step] = piece[: 4 * chans]
+        qf_ref[member, :, start : start + step] = piece[4 * chans :]
+    for k in range(1, members):
+        peer = at(first + lax.rem(member + k, members), t)
+        launch(remote(qf_ref.at[member], qf_ref.at[member], send_q.at[k], recv_q.at[k], peer))
+    for k in range(1, members):
+        there = qf_ref.at[lax.rem(member - k + members, members)]
+        remote(there, there, send_q.at[k], recv_q.at[k], c_peer).wait_recv()
+    for copy in pending:
+        copy.wait_send()
+
+
+def mix_kernel(sizes, p_ref, qf_ref, jump_ref, par_ref, a_ref, q_s, k_s, d_s, r_s):
+    n_sp, chans, members, width, block, part = sizes
+    s = lax.axis_index("sp")
+    total = p_ref.shape[1]
+    f32, bf16 = jnp.float32, jnp.bfloat16
+    mine = par_ref[pl.ds(pl.multiple_of(s * chans, chans), chans), :]
+    head = s // members
+    span = chans * members
+    margin = par_ref[pl.ds(pl.multiple_of(head * span, span), span), width + 1 : width + 2]
+
+    value = p_ref[0:chans, :].astype(f32)
+    gate = p_ref[chans : 2 * chans, :].astype(f32)
+    gated = value * jax.nn.sigmoid(gate)
+    place = lax.broadcasted_iota(jnp.int32, gated.shape, 1)
+    conv = gated * mine[:, width - 1 : width]
+    for back in range(1, width):
+        moved = jnp.where(place >= back, pltpu.roll(gated, back, 1), 0.0)
+        conv = conv + moved * mine[:, width - 1 - back : width - back]
+    a_ref[0:chans, :] = conv.astype(bf16)
+
+    picked = lax.broadcasted_iota(jnp.int32, jump_ref.shape[1:], 0) == head
+    for b in range(n_sp):
+        lanes = slice(b * part, (b + 1) * part)
+        jump = jnp.sum(jnp.where(picked, jump_ref[b], 0.0), axis=0, keepdims=True)
+        both = [qf_ref[m, :, lanes].astype(f32) for m in range(members)]
+        query = jnp.concatenate([v[:chans] for v in both], axis=0)
+        forget = jnp.concatenate([v[chans:] for v in both], axis=0)
+        key = margin * jax.nn.sigmoid(-forget)
+        q_s[lanes, :] = (query * jax.nn.sigmoid(query)).T
+        k_s[lanes, :] = key.T
+        d_s[lanes, :] = (jnp.log1p(-key) + jump).T
+    low = lax.broadcasted_iota(jnp.int32, (block, block), 0) >= lax.broadcasted_iota(
+        jnp.int32, (block, block), 1
+    )
+    tri = low.astype(bf16)
+    inputs = p_ref[2 * chans : 3 * chans, :].astype(f32).T.astype(bf16)
+    state = jnp.zeros((span, chans), f32)
+    for n in range(total // block):
+        at_rows = slice(n * block, (n + 1) * block)
+        decay = d_s[at_rows, :]
+        high = decay.astype(bf16)
+        rest = (decay - high.astype(f32)).astype(bf16)
+        cum = jnp.dot(tri, high, preferred_element_type=f32) + jnp.dot(
+            tri, rest, preferred_element_type=f32
+        )
+        last = cum[block - 1 : block, :]
+        qs = (q_s[at_rows, :] * jnp.exp(cum)).astype(bf16)
+        key = k_s[at_rows, :]
+        ks = (key * jnp.exp(-cum)).astype(bf16)
+        kf = (key * jnp.exp(last - cum)).astype(bf16)
+        rows_in = inputs[at_rows, :]
+        scores = lax.dot_general(qs, ks, NT, preferred_element_type=f32)
+        scores = jnp.where(low, scores, 0.0).astype(bf16)
+        r_s[at_rows, :] = jnp.dot(scores, rows_in, preferred_element_type=f32) + jnp.dot(
+            qs, state.astype(bf16), preferred_element_type=f32
+        )
+        state = jnp.exp(last).T * state + lax.dot_general(
+            kf, rows_in, TN, preferred_element_type=f32
+        )
+    rec = r_s[...].T
+    outgate = p_ref[3 * chans : 4 * chans, :].astype(f32)
+    square = jnp.sum(rec * rec, axis=0, keepdims=True)
+    a_ref[chans : 2 * chans, :] = (
+        rec * mine[:, width : width + 1] * (outgate * jax.nn.sigmoid(outgate))
+    ).astype(bf16)
+    upper = square.astype(bf16).astype(f32)
+    line = lax.broadcasted_iota(jnp.int32, (a_ref.shape[0] - 2 * chans, total), 0)
+    a_ref[2 * chans :, :] = jnp.where(
+        line == 0, upper, jnp.where(line == 1, square - upper, 0.0)
+    ).astype(bf16)
+
+
+def output_kernel(
+    sizes, a_ref, wo_ref, par_ref, o_ref, held, sums, part, got, mixed, *sems
+):
+    n_sp, n_tp, rows, chans, members, width, channels = sizes
+    send_z, send_x, recv_z, recv_x, send_s, recv_s, send_p, recv_p, send_o, recv_o = sems
+    f32, bf16 = jnp.float32, jnp.bfloat16
+    s, t = lax.axis_index("sp"), lax.axis_index("tp")
+    n_z = n_sp // STRIDE
+    z, x = s // STRIDE, s % STRIDE
+    x_peer = at(z * STRIDE + (1 - x), t)
+
+    def sp_at(k):
+        return lax.rem(s + k, n_sp)
+
+    def tp_at(k):
+        return lax.rem(t + k, n_tp)
+
+    greet([at(sp_at(k), t) for k in range(1, n_sp)] + [at(s, tp_at(k)) for k in range(1, n_tp)])
+    pending = []
+
+    def launch(copy):
+        copy.start()
+        pending.append(copy)
+
+    for k in range(1, n_z):
+        peer = at(lax.rem(z + k, n_z) * STRIDE + x, t)
+        launch(remote(a_ref, held.at[s], send_z.at[k], recv_z.at[k], peer))
+    launch(remote(a_ref, held.at[s], send_x.at[0], recv_x.at[0], x_peer))
+    held[s] = a_ref[...]
+    for k in range(1, n_z):
+        source = lax.rem(z - k + n_z, n_z) * STRIDE + x
+        here = held.at[source]
+        remote(here, here, send_z.at[k], recv_z.at[k], x_peer).wait_recv()
+        launch(remote(here, here, send_x.at[k], recv_x.at[k], x_peer))
+    for k in range(n_z):
+        here = held.at[lax.rem(z - k + n_z, n_z) * STRIDE + (1 - x)]
+        remote(here, here, send_x.at[k], recv_x.at[k], x_peer).wait_recv()
+
+    total = a_ref.shape[1]
+    conv = held[:, 0:chans, :].reshape(n_sp * chans, total).astype(f32)
+    sums[t, 0:1, :] = jnp.sum(conv, axis=0, keepdims=True)
+    sums[t, 1:2, :] = jnp.sum(conv * conv, axis=0, keepdims=True)
+    for k in range(1, n_tp):
+        launch(remote(sums.at[t], sums.at[t], send_s.at[k], recv_s.at[k], at(s, tp_at(k))))
+    for k in range(1, n_tp):
+        there = sums.at[lax.rem(t - k + n_tp, n_tp)]
+        remote(there, there, send_s.at[k], recv_s.at[k], x_peer).wait_recv()
+    both = sums[0]
+    for k in range(1, n_tp):
+        both = both + sums[k]
+    mean = both[0:1] / channels
+    scale = lax.rsqrt(both[1:2] / channels - mean * mean + layer_eps)
+    gain = par_ref[:, width + 2 : width + 3]
+    bias = par_ref[:, width + 3 : width + 4]
+    span = members * chans
+    heads = n_sp // members
+    step = rows * n_tp
+    for b in range(n_sp):
+        lanes = slice(b * step, (b + 1) * step)
+        values = held[:, 0:chans, lanes].reshape(n_sp * chans, step).astype(f32)
+        shifted = (values - mean[:, lanes]) * scale[:, lanes] * gain + bias
+        pieces = [(shifted * jax.nn.sigmoid(shifted)).astype(bf16)]
+        for h in range(heads):
+            group = slice(h * members, (h + 1) * members)
+            square = jnp.sum(held[group, 2 * chans : 2 * chans + 16, lanes].astype(f32), axis=(0, 1), keepdims=True)[0]
+            ups = held[group, chans : 2 * chans, lanes].reshape(span, step).astype(f32)
+            pieces.append((ups * lax.rsqrt(square / span + norm_eps)).astype(bf16))
+        out = lax.dot_general(
+            jnp.concatenate(pieces, axis=0), wo_ref[...], TN, preferred_element_type=f32
+        ).astype(bf16)
+        for k in range(n_tp):
+            part[k, b * rows : (b + 1) * rows, :] = out[k * rows : (k + 1) * rows]
+    for k in range(1, n_tp):
+        launch(remote(part.at[tp_at(k)], got.at[k], send_p.at[k], recv_p.at[k], at(s, tp_at(k))))
+    added = part[t].astype(f32)
+    for k in range(1, n_tp):
+        remote(got.at[k], got.at[k], send_p.at[k], recv_p.at[k], x_peer).wait_recv()
+        added = added + got[k].astype(f32)
+    mixed[...] = added.astype(bf16)
+    cols = wo_ref.shape[1]
+
+    def window(source):
+        return o_ref.at[:, pl.ds(pl.multiple_of(source * cols, cols), cols)]
+
+    def block_of(sp):
+        return pl.ds(pl.multiple_of(sp * rows, rows), rows)
+
+    for k in range(1, n_sp):
+        launch(remote(mixed.at[block_of(sp_at(k))], window(s), send_o.at[k], recv_o.at[k], at(sp_at(k), t)))
+    window(s)[...] = mixed[block_of(s), :]
+    for k in range(1, n_sp):
+        there = window(lax.rem(s - k + n_sp, n_sp))
+        remote(there, there, send_o.at[k], recv_o.at[k], x_peer).wait_recv()
+    for copy in pending:
+        copy.wait_send()
+
+
+def spread_channels(n_sp, n_tp,
+    tokens,
+    input_norm_gain,
+    convolution_value_weight,
+    convolution_gate_weight,
+    depthwise_filter_taps,
+    channel_norm_gain,
+    channel_norm_bias,
+    query_projection_weight,
+    forget_gate_weight,
+    recurrence_value_weight,
+    output_gate_weight,
+    forget_floor_margin,
+    decay_jump_terms,
+    head_norm_gain,
+    convolution_output_weight,
+    recurrence_output_weight,
+):
+    rows, model = tokens.shape
+    total = rows * n_sp * n_tp
+    depth, group_chans = convolution_value_weight.shape
+    chans = group_chans // n_sp
+    heads, part = decay_jump_terms.shape
+    members = n_sp // heads
+    width = depthwise_filter_taps.shape[0]
+    features = tokens.astype(jnp.float32)
+    normed = (
+        features
+        * lax.rsqrt(jnp.mean(features * features, axis=1, keepdims=True) + norm_eps)
+        * input_norm_gain
+    ).astype(jnp.bfloat16)
+    kinds = (
+        convolution_value_weight,
+        convolution_gate_weight,
+        recurrence_value_weight,
+        output_gate_weight,
+        query_projection_weight,
+        forget_gate_weight,
+    )
+    stacked = jnp.stack([w.T.reshape(n_sp, chans, depth) for w in kinds], axis=1).reshape(
+        n_sp, len(kinds) * chans, depth
+    )
+    jumps = jnp.pad(decay_jump_terms, ((0, -heads % 8), (0, 0)))
+    params = jnp.concatenate(
+        [
+            depthwise_filter_taps.T,
+            head_norm_gain[:, None],
+            forget_floor_margin[:, None],
+            channel_norm_gain[:, None],
+            channel_norm_bias[:, None],
+        ],
+        axis=1,
+    )
+    weights_out = jnp.concatenate([convolution_output_weight, recurrence_output_weight], axis=0)
+    vmem = pl.BlockSpec(memory_space=pltpu.VMEM)
+    dma = pltpu.SemaphoreType.DMA
+    bf16, f32 = jnp.bfloat16, jnp.float32
+    n_z = n_sp // STRIDE
+    lanes = 2 * n_sp
+    projected, query_forget, all_jumps = pl.pallas_call(
+        functools.partial(project_kernel, (n_sp, n_tp, rows, depth, chans, members)),
+        out_shape=(
+            jax.ShapeDtypeStruct((4 * chans, total), bf16),
+            jax.ShapeDtypeStruct((members, 2 * chans, total), bf16),
+            jax.ShapeDtypeStruct((n_sp, *jumps.shape), f32),
+        ),
+        in_specs=[vmem] * 3,
+        out_specs=(vmem,) * 3,
+        scratch_shapes=[
+            pltpu.VMEM((total, model), bf16),
+            pltpu.VMEM((len(kinds) * chans, model), bf16),
+            dma((n_z,)),
+            dma((n_z,)),
+            dma((lanes,)),
+            dma((lanes,)),
+            dma((lanes,)),
+            dma((lanes,)),
+            dma((n_sp,)),
+            dma((n_sp,)),
+            dma((n_sp,)),
+            dma((n_sp,)),
+            dma((members,)),
+            dma((members,)),
+        ],
+        compiler_params=pltpu.CompilerParams(collective_id=0, has_side_effects=True),
+        name="project",
+    )(normed, stacked, jumps)
+    span = members * chans
+    sent = pl.pallas_call(
+        functools.partial(mix_kernel, (n_sp, chans, members, width, HG_BLOCK, part)),
+        out_shape=jax.ShapeDtypeStruct((2 * chans + 16, total), bf16),
+        in_specs=[vmem] * 4,
+        out_specs=vmem,
+        scratch_shapes=[pltpu.VMEM((total, span), f32)] * 3 + [pltpu.VMEM((total, chans), f32)],
+        name="mix",
+    )(projected, query_forget, all_jumps, params)
+    cols = weights_out.shape[1]
+    return pl.pallas_call(
+        functools.partial(
+            output_kernel, (n_sp, n_tp, rows, chans, members, width, group_chans * n_tp)
+        ),
+        out_shape=jax.ShapeDtypeStruct((rows, model), bf16),
+        in_specs=[vmem] * 3,
+        out_specs=vmem,
+        scratch_shapes=[
+            pltpu.VMEM((n_sp, 2 * chans + 16, total), bf16),
+            pltpu.VMEM((n_tp, 8, total), f32),
+            pltpu.VMEM((n_tp, n_sp * rows, cols), bf16),
+            pltpu.VMEM((n_tp, n_sp * rows, cols), bf16),
+            pltpu.VMEM((n_sp * rows, cols), bf16),
+            dma((n_z,)),
+            dma((n_z,)),
+            dma((n_z,)),
+            dma((n_z,)),
+            dma((n_tp,)),
+            dma((n_tp,)),
+            dma((n_tp,)),
+            dma((n_tp,)),
+            dma((n_sp,)),
+            dma((n_sp,)),
+        ],
+        compiler_params=pltpu.CompilerParams(collective_id=1, has_side_effects=True),
+        name="output",
+    )(sent, weights_out, params)
+
+
+def layer(n_sp, n_tp, *arrays):
+    rows, model = arrays[0].shape
+    group_chans = arrays[2].shape[1]
+    heads = arrays[12].shape[0]
+    gathered_bytes = rows * n_sp * n_tp * model * arrays[0].dtype.itemsize
+    fits = gathered_bytes <= 2**23
+    even = n_tp == 4 and n_sp % heads == 0 and n_sp % STRIDE == 0 and group_chans % (32 * n_sp) == 0
+    if fits and even:
+        return spread_channels(n_sp, n_tp, *arrays)
+    return per_device(*arrays)
+
+
 def solution(mesh):
     in_specs = (
         P(("sp", "tp"), None),
@@ -248,5 +684,5 @@
     )
     out_specs = P(("sp", "tp"), None)
     return jax.shard_map(
-        per_device, mesh=mesh, in_specs=in_specs, out_specs=out_specs, check_vma=False
-    )
+        functools.partial(layer, mesh.shape["sp"], mesh.shape["tp"]), mesh=mesh, in_specs=in_specs, out_specs=out_specs, check_vma=False
+    )

time: 372 us -> 118 us (0.32)
  waiting for transfers between devices: 266 us -> 0 us
  Pallas kernels: 0 us -> 104 us
  blocking collectives: 64.7 us -> 0 us
  matrix products: 16.3 us -> 0 us
  between operations: 13.5 us -> 0.21 us
  local copies, waits for them, and re-layouts: 3.35 us -> 11.1 us
  starting transfers between devices: 5.28 us -> 0 us
    all_gather x8 -> x0, waiting for transfers between devices: 240 us -> none  [the longest x1 40.2 us: per_device(): lax.all_gather(recurrence_output_weight, 'sp', axis=1, tiled=True)]
    pallas_call x0 -> x3, Pallas kernels: none -> 104 us  [the longest x1 52.6 us: spread_channels(): pl.pallas_call(functools.partial(project_kernel, (n_sp, n_tp, rows, depth...]
    all_gather x3 -> x0, blocking collectives: 59 us -> none  [the longest x2 50.3 us: prefix(): lax.all_gather(part.astype(kind), axis)]
    reduce_scatter x1 -> x0, waiting for transfers between devices: 20.9 us -> none  [per_device(): lax.psum_scatter((jnp.dot(conv_part, conv_columns, preferred_element_type...]
    dot_general x11 -> x0, matrix products: 14.1 us -> none  [the longest x5 7.87 us: project(): jnp.dot(row_piece, weight, preferred_element_type=jnp.float32)]
    unnamed x16 -> x42, local copies, waits for them, and re-layouts: 2.59 us -> 8.73 us
    psum x1 -> x0, blocking collectives: 5.67 us -> none  [per_device(): lax.psum((jnp.sum(values, axis=1), jnp.sum(values * values, axis=1)), 'tp')]
    unnamed x9 -> x0, waiting for transfers between devices: 5.07 us -> none
  transfers between devices with their start and end apart: 11 -> 0, of which waited for: 8 -> 0; matrix products, arithmetic and copies ran while one was open for 4% -> 0% of each run, Pallas kernels for 0% -> 0%
where the time goes in v1:
time: 118 us; the launch traced here: 117 us
  Pallas kernels  104 us (88%)
  local copies, waits for them, and re-layouts  11.1 us (9%)
  other arithmetic  1.61 us (1%)
    pallas_call x1, Pallas kernels, spread_channels(): pl.pallas_call(functools.partial(project_kernel, (n_sp, n_tp, rows, depth...  52.6 us
    pallas_call x1, Pallas kernels, spread_channels(): pl.pallas_call(functools.partial(output_kernel, (n_sp, n_tp, rows, chans,...  44.9 us
    unnamed x42, local copies, waits for them, and re-layouts  8.73 us
    pallas_call x1, Pallas kernels, spread_channels(): pl.pallas_call(functools.partial(mix_kernel, (n_sp, chans, members, width...  6.61 us

profile of v1, /device:TPU:0, one launch (start us, length us, event | category | flops | bytes accessed | tf_op | source)
XLA Modules:
  0.0 117.1 jit_solution(17571075928418978471)
XLA Ops:
  0.0 1.0 copy.36
  1.0 0.0 copy-start.1
  1.0 0.9 copy-done.1
  1.9 0.1 copy.37
  2.0 0.0 copy-start.2
  2.1 0.9 copy-done.2
  2.9 0.1 copy.38
  3.0 0.0 copy-start.3
  3.1 0.9 copy-done.3
  3.9 0.1 copy.39
  4.0 0.0 copy-start.4
  4.1 0.9 copy-done.4
  5.0 0.1 copy.40
  5.1 0.0 copy-start.5
  5.1 0.9 copy-done.5
  6.0 0.1 copy.41
  6.1 0.0 copy-start
  6.1 1.0 copy.42
  7.1 0.0 copy-done
  7.1 0.0 copy-start.9
  7.1 0.1 fusion
  7.2 0.5 copy-done.9
  7.8 0.0 copy-start.14
  7.8 0.8 fusion.2.x_ref
  8.5 0.0 copy-done.14
  8.5 0.6 pad.4.j_ref
  9.1 0.0 copy-start.8
  9.1 0.0 copy-start.11
  9.1 0.0 copy-start.12
  9.1 0.0 copy-start.13
  9.1 52.6 %project.1 = (bf16[128,1024]{1,0:T(8,128)(2,1)}, bf16[4,64,1024]{2,1,0:T(8,128)(2,1)}, f32[8,8,128]{2,1,0:T(8,128)}) custom-call(bf16[32,2048]{1,0:T(8,128)(2,1)} %fusion.2.x_ref, bf16[8,192,256]{2,1,0:T(8,128)(2,1)} %bitcast.24, f32[8,128]{1,0:T(8,128)} %pad.4.j_ref), custom_call_target="tpu_custom_call" | custom-call | tf_op jit(solution)/shard_map/project/pallas_call | solution.py:587
  61.8 0.0 copy-start.10
  61.8 0.0 copy-done.8
  61.8 0.0 copy-done.11
  61.8 0.0 copy-done.12
  61.8 0.0 copy-done.13
  61.8 0.6 copy-done.10
  62.5 0.8 copy.43.par_ref
  63.3 0.0 copy-start.6
  63.3 0.0 copy-start.7
  63.3 6.6 %mix.1.a_ref = bf16[80,1024]{1,0:T(8,128)(2,1)} custom-call(bf16[128,1024]{1,0:T(8,128)(2,1)} %get-tuple-element.8.p_ref, bf16[4,64,1024]{2,1,0:T(8,128)(2,1)} %get-tuple-element.9.qf_ref, f32[8,8,128]{2,1,0:T(8,128)} %get-tuple-element.10.jump_ref, f32[256,35]{1,0:T(8,128)} %copy.43.par_ref), custom_call_target="tpu_custom_call" | custom-call | tf_op jit(solution)/shard_map/mix/pallas_call | solution.py:616
  69.9 0.0 copy-done.6
  69.9 0.0 copy-done.7
  69.9 0.7 pad_maximum_fusion.wo_ref
  70.6 44.9 %output.1 = bf16[32,2048]{1,0:T(8,128)(2,1)} custom-call(bf16[80,1024]{1,0:T(8,128)(2,1)} %mix.1.a_ref, bf16[512,256]{1,0:T(8,128)(2,1)} %pad_maximum_fusion.wo_ref, f32[256,35]{1,0:T(8,128)} %copy.43.par_ref), custom_call_target="tpu_custom_call" | custom-call | tf_op jit(solution)/shard_map/output/pallas_call | solution.py:625
  115.5 1.6 %copy.51 = bf16[32,2048]{1,0:T(8,128)(2,1)} copy(bf16[32,2048]{1,0:T(8,128)(2,1)} %output.1) | data formatting | bytes 262144
  (8 shorter events, 0.1 us)
Async XLA Ops:
  1.0 0.9 copy-start.1
  2.0 0.9 copy-start.2
  3.0 0.9 copy-start.3
  4.0 0.9 copy-start.4
  5.1 0.9 copy-start.5
  6.1 1.0 copy-start
  7.1 0.7 copy-start.9
  7.8 0.8 copy-start.14
  9.1 52.7 %copy-start.8 = (f32[31,256]{1,0:T(8,128)S(1)}, f32[31,256]{1,0:T(8,128)}, u32[]{:S(2)}) copy-start(f32[31,256]{1,0:T(8,128)} %param.20) | copy-start | bytes 95236
  9.1 52.7 %copy-start.11 = (f32[256]{0:T(256)S(1)}, f32[256]{0:T(256)}, u32[]{:S(2)}) copy-start(f32[256]{0:T(256)} %param.27) | copy-start | bytes 3076
  9.1 52.7 %copy-start.12 = (f32[256]{0:T(256)S(1)}, f32[256]{0:T(256)}, u32[]{:S(2)}) copy-start(f32[256]{0:T(256)} %param.21) | copy-start | bytes 3076
  9.1 52.7 %copy-start.13 = (f32[256]{0:T(256)S(1)}, f32[256]{0:T(256)}, u32[]{:S(2)}) copy-start(f32[256]{0:T(256)} %param.22) | copy-start | bytes 3076
  61.8 0.7 copy-start.10
  63.3 6.6 %copy-start.6 = (bf16[256,256]{1,0:T(8,128)(2,1)S(1)}, bf16[256,256]{1,0:T(8,128)(2,1)}, u32[]{:S(2)}) copy-start(bf16[256,256]{1,0:T(8,128)(2,1)} %param.31) | copy-start | bytes 393220
  63.3 6.6 %copy-start.7 = (bf16[256,256]{1,0:T(8,128)(2,1)S(1)}, bf16[256,256]{1,0:T(8,128)(2,1)}, u32[]{:S(2)}) copy-start(bf16[256,256]{1,0:T(8,128)(2,1)} %param.30) | copy-start | bytes 393220

commit v2 on v1

--- a/solution.py
+++ b/solution.py
@@ -255,7 +255,8 @@
 
 
 def project_kernel(
-    sizes, x_ref, w_ref, j_ref, p_ref, qf_ref, jump_ref, held, weights, *sems
+    sizes, x_hbm, gain_ref, j_ref, cv, cg, rv, og, qw, fw, p_ref, qf_ref, jump_ref,
+    x_ref, raw, w_ref, held, weights, load, *sems
 ):
     n_sp, n_tp, rows, depth, chans, members = sizes
     (send_z, send_x, send_y, send_c, lane, sib, send_w, recv_w, send_j, recv_j, send_q, recv_q) = sems
@@ -266,6 +267,8 @@
     x_peer = at(z * STRIDE + (1 - x), t)
     y_peer = at(s, (1 - y) * 2 + c)
     c_peer = at(s, y * 2 + (1 - c))
+    total = held.shape[0]
+    half = total // 2
 
     def sp_peer(k):
         return lax.rem(s + k, n_sp)
@@ -274,86 +277,145 @@
         from_z = lax.rem(z - dz + n_z, n_z)
         from_x = (1 - x) if dx else x
         from_y = (1 - y) if dy else y
-        shard = (from_z * STRIDE + from_x) * n_tp + from_y * 2 + core
-        return pl.ds(pl.multiple_of(shard * rows, rows), rows)
+        start = from_y * half + ((from_z * STRIDE + from_x) * 2 + core) * rows
+        return pl.ds(pl.multiple_of(start, rows), rows)
 
     def number(dy, dx, dz):
         return (dy * STRIDE + dx) * n_z + dz
 
-    greet([at(sp_peer(k), t) for k in range(1, n_sp)] + [y_peer, c_peer])
+    peers = [at(sp_peer(k), t) for k in range(1, n_sp)] + [y_peer, c_peer]
+    barrier = pltpu.get_barrier_semaphore()
+    for peer in peers:
+        pl.semaphore_signal(barrier, inc=1, device_id=peer, device_id_type=MESH)
+    kinds = (cv, cg, rv, og, qw, fw)
+    loads = [pltpu.make_async_copy(x_hbm, x_ref, load.at[0])] + [
+        pltpu.make_async_copy(w, raw.at[i], load.at[1 + i]) for i, w in enumerate(kinds)
+    ]
+    for copy in loads:
+        copy.start()
+    own = slot(0, 0, 0, c)
+    mine = held.at[own]
+    loads[0].wait()
+    features = x_ref[...].astype(jnp.float32)
+    mine[...] = (
+        features
+        * lax.rsqrt(jnp.mean(features * features, axis=1, keepdims=True) + norm_eps)
+        * gain_ref[...]
+    ).astype(jnp.bfloat16)
+    pl.semaphore_wait(barrier, len(peers))
     pending = []
 
     def launch(copy):
         copy.start()
         pending.append(copy)
 
-    own = slot(0, 0, 0, c)
-
-    def pass_on(dy, dx, dz, src):
-        here = slot(dy, dx, dz, c)
+    def pass_on(dy, dx, dz):
+        here = held.at[slot(dy, dx, dz, c)]
         at_number = number(dy, dx, dz)
         if not dy:
             if not dx:
-                launch(remote(src, held.at[here], send_x.at[dz], lane.at[number(0, 1, dz)], x_peer))
-            launch(remote(src, held.at[here], send_y.at[at_number], lane.at[number(1, dx, dz)], y_peer))
-        launch(remote(src, held.at[here], send_c.at[at_number], sib.at[at_number], c_peer))
-
-    for k in range(1, n_z):
+                launch(remote(here, here, send_x.at[dz], lane.at[number(0, 1, dz)], x_peer))
+            launch(remote(here, here, send_y.at[at_number], lane.at[number(1, dx, dz)], y_peer))
+        launch(remote(here, here, send_c.at[at_number], sib.at[at_number], c_peer))
+
+    near_first = sorted(range(1, n_z), key=lambda k: min(k, n_z - k))
+    for k in near_first:
         peer = at(lax.rem(z + k, n_z) * STRIDE + x, t)
-        launch(remote(x_ref, held.at[own], send_z.at[k], lane.at[k], peer))
-    pass_on(0, 0, 0, x_ref)
-    my_columns = pl.ds(pl.multiple_of(s * depth, depth), depth)
+        launch(remote(mine, mine, send_z.at[k], lane.at[k], peer))
+    pass_on(0, 0, 0)
     for k in range(1, n_sp):
         launch(remote(j_ref, jump_ref.at[s], send_j.at[k], recv_j.at[k], at(sp_peer(k), t)))
-    for k in range(1, n_sp):
-        launch(
-            remote(w_ref.at[sp_peer(k)], weights.at[:, my_columns], send_w.at[k], recv_w.at[k], at(sp_peer(k), t))
-        )
-    held[own, :] = x_ref[...]
     jump_ref[s] = j_ref[...]
+    for i in range(len(kinds)):
+        loads[1 + i].wait()
+        turned = raw[i].T
+        for d in range(n_sp):
+            w_ref[d, i * chans : (i + 1) * chans, :] = turned[d * chans : (d + 1) * chans]
+    my_columns = pl.ds(pl.multiple_of(s * depth, depth), depth)
+
+    def send_weights(dx, dz):
+        other = lax.rem(z + dz, n_z) * STRIDE + ((1 - x) if dx else x)
+        k = dx * n_z + dz
+        launch(remote(w_ref.at[other], weights.at[:, my_columns], send_w.at[k], recv_w.at[k], at(other, t)))
+
+    for dz in near_first:
+        send_weights(0, dz)
     weights[:, my_columns] = w_ref[s]
 
     def arrived(dy, dx, dz):
         here = held.at[slot(dy, dx, dz, c)]
         remote(here, here, send_c.at[0], lane.at[number(dy, dx, dz)], c_peer).wait_recv()
-        pass_on(dy, dx, dz, here)
-
-    for dz in range(1, n_z):
-        arrived(0, 0, dz)
-    for dz in range(n_z):
-        arrived(0, 1, dz)
+        pass_on(dy, dx, dz)
+
+    order = []
+    for dz in near_first:
+        order += [(0, dz), (1, 0 if dz == near_first[0] else order[-2][1])]
+    order.append((1, near_first[-1]))
+    for dx, dz in order:
+        arrived(0, dx, dz)
+    for dz in [0] + near_first:
+        send_weights(1, dz)
+    across = [(0, 0)] + order
+    early = len(across) // 2 + 1
+    for dx, dz in across[:early]:
+        arrived(1, dx, dz)
     for dx in range(STRIDE):
         for dz in range(n_z):
-            arrived(1, dx, dz)
-    for k in range(1, n_sp):
-        source = lax.rem(s - k + n_sp, n_sp)
-        there = weights.at[:, pl.ds(pl.multiple_of(source * depth, depth), depth)]
-        remote(there, there, send_w.at[k], recv_w.at[k], c_peer).wait_recv()
-        remote(j_ref, jump_ref.at[source], send_j.at[k], recv_j.at[k], c_peer).wait_recv()
-    for dy in range(2):
+            if dx or dz:
+                source = lax.rem(z - dz + n_z, n_z) * STRIDE + ((1 - x) if dx else x)
+                there = weights.at[:, pl.ds(pl.multiple_of(source * depth, depth), depth)]
+                k = dx * n_z + dz
+                remote(there, there, send_w.at[k], recv_w.at[k], c_peer).wait_recv()
+    member = lax.rem(s, members)
+    first = s - member
+
+    def project_half(dy):
         for dx in range(STRIDE):
             for dz in range(n_z):
                 here = held.at[slot(dy, dx, dz, 1 - c)]
                 remote(here, here, send_c.at[0], sib.at[number(dy, dx, dz)], c_peer).wait_recv()
-
-    member = lax.rem(s, members)
-    first = s - member
-    total = held.shape[0]
-    step = min(256, total)
-    for start in range(0, total, step):
-        piece = lax.dot_general(
-            held[start : start + step, :], weights[...], NT, preferred_element_type=jnp.float32
-        ).T.astype(jnp.bfloat16)
-        p_ref[:, start : start + step] = piece[: 4 * chans]
-        qf_ref[member, :, start : start + step] = piece[4 * chans :]
-    for k in range(1, members):
-        peer = at(first + lax.rem(member + k, members), t)
-        launch(remote(qf_ref.at[member], qf_ref.at[member], send_q.at[k], recv_q.at[k], peer))
-    for k in range(1, members):
-        there = qf_ref.at[lax.rem(member - k + members, members)]
-        remote(there, there, send_q.at[k], recv_q.at[k], c_peer).wait_recv()
+        base = ((1 - y) if dy else y) * half
+        step = min(256, half)
+        for start in range(0, half, step):
+            span = pl.ds(pl.multiple_of(base + start, step), step)
+            piece = lax.dot_general(
+                held[span, :], weights[...], NT, preferred_element_type=jnp.float32
+            ).T.astype(jnp.bfloat16)
+            qf_ref[member, :, span] = piece[4 * chans :]
+            p_ref[:, span] = piece[: 4 * chans]
+        window = pl.ds(pl.multiple_of(base, half), half)
+        for k in range(1, members):
+            peer = at(first + lax.rem(member + k, members), t)
+            block = qf_ref.at[member, :, window]
+            launch(remote(block, block, send_q.at[dy, k], recv_q.at[dy, k], peer))
+
+    project_half(0)
+    for dx, dz in across[early:]:
+        arrived(1, dx, dz)
+    project_half(1)
+    for dy in range(2):
+        window = pl.ds(pl.multiple_of(((1 - y) if dy else y) * half, half), half)
+        for k in range(1, members):
+            there = qf_ref.at[lax.rem(member - k + members, members), :, window]
+            remote(there, there, send_q.at[dy, k], recv_q.at[dy, k], c_peer).wait_recv()
+    for k in range(1, n_sp):
+        there = jump_ref.at[lax.rem(s - k + n_sp, n_sp)]
+        remote(there, there, send_j.at[k], recv_j.at[k], c_peer).wait_recv()
     for copy in pending:
         copy.wait_send()
+
+
+def in_order(array, n_sp):
+    half = array.shape[1] // 2
+    own = half // n_sp
+    return jnp.concatenate(
+        [
+            array[:, side * half + b * own : side * half + (b + 1) * own]
+            for b in range(n_sp)
+            for side in range(2)
+        ],
+        axis=1,
+    )
 
 
 def mix_kernel(sizes, p_ref, qf_ref, jump_ref, par_ref, a_ref, q_s, k_s, d_s, r_s):
@@ -366,8 +428,9 @@
     span = chans * members
     margin = par_ref[pl.ds(pl.multiple_of(head * span, span), span), width + 1 : width + 2]
 
-    value = p_ref[0:chans, :].astype(f32)
-    gate = p_ref[chans : 2 * chans, :].astype(f32)
+    projected = in_order(p_ref[...].astype(f32), n_sp)
+    value = projected[0:chans]
+    gate = projected[chans : 2 * chans]
     gated = value * jax.nn.sigmoid(gate)
     place = lax.broadcasted_iota(jnp.int32, gated.shape, 1)
     conv = gated * mine[:, width - 1 : width]
@@ -377,10 +440,11 @@
     a_ref[0:chans, :] = conv.astype(bf16)
 
     picked = lax.broadcasted_iota(jnp.int32, jump_ref.shape[1:], 0) == head
+    arranged = [in_order(qf_ref[m].astype(f32), n_sp) for m in range(members)]
     for b in range(n_sp):
         lanes = slice(b * part, (b + 1) * part)
         jump = jnp.sum(jnp.where(picked, jump_ref[b], 0.0), axis=0, keepdims=True)
-        both = [qf_ref[m, :, lanes].astype(f32) for m in range(members)]
+        both = [arranged[m][:, lanes] for m in range(members)]
         query = jnp.concatenate([v[:chans] for v in both], axis=0)
         forget = jnp.concatenate([v[chans:] for v in both], axis=0)
         key = margin * jax.nn.sigmoid(-forget)
@@ -391,7 +455,7 @@
         jnp.int32, (block, block), 1
     )
     tri = low.astype(bf16)
-    inputs = p_ref[2 * chans : 3 * chans, :].astype(f32).T.astype(bf16)
+    inputs = projected[2 * chans : 3 * chans].T.astype(bf16)
     state = jnp.zeros((span, chans), f32)
     for n in range(total // block):
         at_rows = slice(n * block, (n + 1) * block)
@@ -416,7 +480,7 @@
             kf, rows_in, TN, preferred_element_type=f32
         )
     rec = r_s[...].T
-    outgate = p_ref[3 * chans : 4 * chans, :].astype(f32)
+    outgate = projected[3 * chans : 4 * chans]
     square = jnp.sum(rec * rec, axis=0, keepdims=True)
     a_ref[chans : 2 * chans, :] = (
         rec * mine[:, width : width + 1] * (outgate * jax.nn.sigmoid(outgate))
@@ -550,12 +614,6 @@
     heads, part = decay_jump_terms.shape
     members = n_sp // heads
     width = depthwise_filter_taps.shape[0]
-    features = tokens.astype(jnp.float32)
-    normed = (
-        features
-        * lax.rsqrt(jnp.mean(features * features, axis=1, keepdims=True) + norm_eps)
-        * input_norm_gain
-    ).astype(jnp.bfloat16)
     kinds = (
         convolution_value_weight,
         convolution_gate_weight,
@@ -563,9 +621,6 @@
         output_gate_weight,
         query_projection_weight,
         forget_gate_weight,
-    )
-    stacked = jnp.stack([w.T.reshape(n_sp, chans, depth) for w in kinds], axis=1).reshape(
-        n_sp, len(kinds) * chans, depth
     )
     jumps = jnp.pad(decay_jump_terms, ((0, -heads % 8), (0, 0)))
     params = jnp.concatenate(
@@ -580,6 +635,7 @@
     )
     weights_out = jnp.concatenate([convolution_output_weight, recurrence_output_weight], axis=0)
     vmem = pl.BlockSpec(memory_space=pltpu.VMEM)
+    anywhere = pl.BlockSpec(memory_space=pl.ANY)
     dma = pltpu.SemaphoreType.DMA
     bf16, f32 = jnp.bfloat16, jnp.float32
     n_z = n_sp // STRIDE
@@ -591,11 +647,15 @@
             jax.ShapeDtypeStruct((members, 2 * chans, total), bf16),
             jax.ShapeDtypeStruct((n_sp, *jumps.shape), f32),
         ),
-        in_specs=[vmem] * 3,
+        in_specs=[anywhere, vmem, vmem] + [anywhere] * len(kinds),
         out_specs=(vmem,) * 3,
         scratch_shapes=[
+            pltpu.VMEM((rows, model), bf16),
+            pltpu.VMEM((len(kinds), depth, group_chans), bf16),
+            pltpu.VMEM((n_sp, len(kinds) * chans, depth), bf16),
             pltpu.VMEM((total, model), bf16),
             pltpu.VMEM((len(kinds) * chans, model), bf16),
+            dma((1 + len(kinds),)),
             dma((n_z,)),
             dma((n_z,)),
             dma((lanes,)),
@@ -606,12 +666,12 @@
             dma((n_sp,)),
             dma((n_sp,)),
             dma((n_sp,)),
-            dma((members,)),
-            dma((members,)),
+            dma((2, members)),
+            dma((2, members)),
         ],
         compiler_params=pltpu.CompilerParams(collective_id=0, has_side_effects=True),
         name="project",
-    )(normed, stacked, jumps)
+    )(tokens, input_norm_gain[None, :], jumps, *kinds)
     span = members * chans
     sent = pl.pallas_call(
         functools.partial(mix_kernel, (n_sp, chans, members, width, HG_BLOCK, part)),

time: 118 us -> 104 us (0.88)
  Pallas kernels: 104 us -> 97.1 us
  local copies, waits for them, and re-layouts: 11.1 us -> 4.35 us
    unnamed x42 -> x15, local copies, waits for them, and re-layouts: 8.73 us -> 2.27 us
    pallas_call x1, Pallas kernels: 52.6 us -> 46.7 us  [spread_channels(): pl.pallas_call(functools.partial(project_kernel, (n_sp, n_tp, rows, depth...]
where the time goes in v2:
time: 104 us; the launch traced here: 102 us
  Pallas kernels  97.1 us (93%)
  local copies, waits for them, and re-layouts  4.35 us (4%)
    pallas_call x1, Pallas kernels, spread_channels(): pl.pallas_call(functools.partial(project_kernel, (n_sp, n_tp, rows, depth...  46.7 us
    pallas_call x1, Pallas kernels, spread_channels(): pl.pallas_call(functools.partial(output_kernel, (n_sp, n_tp, rows, chans,...  43.8 us
    pallas_call x1, Pallas kernels, spread_channels(): pl.pallas_call(functools.partial(mix_kernel, (n_sp, chans, members, width...  6.72 us
    unnamed x15, local copies, waits for them, and re-layouts  2.27 us

profile of v2, /device:TPU:0, one launch (start us, length us, event | category | flops | bytes accessed | tf_op | source)
XLA Modules:
  0.0 102.3 jit_solution(7645428352527504905)
XLA Ops:
  0.0 1.3 %pad.4.j_ref = f32[8,128]{1,0:T(8,128)} pad(f32[2,128]{1,0:T(2,128)} %param.28, f32[]{:T(128)} %constant.2.clone.1), padding=0_6x0_0 | pad | bytes 5124 | tf_op jit(solution)/shard_map/jit(_pad)/pad | solution.py:625
  1.3 0.0 copy-start.2
  1.3 46.7 %project.1 = (bf16[128,1024]{1,0:T(8,128)(2,1)}, bf16[4,64,1024]{2,1,0:T(8,128)(2,1)}, f32[8,8,128]{2,1,0:T(8,128)}) custom-call(bf16[32,2048]{1,0:T(8,128)(2,1)} %x_hbm.1, f32[1,2048]{1,0:T(1,128)} %bitcast.7, f32[8,128]{1,0:T(8,128)} %pad.4.j_ref, bf16[256,256]{1,0:T(8,128)(2,1)} %cv.1, bf16[256,256]{1,0:T(8,128)(2,1)} %cg.1, bf16[256,256]{1,0:T(8,128)(2,1)} %rv.1, ...), custom_call_target="tpu_custom_call" | custom-call | tf_op jit(solution)/shard_map/project/pallas_call | solution.py:643
  47.9 0.0 copy-start.4
  48.0 0.0 copy-start.5
  48.0 0.0 copy-start.6
  48.0 0.0 copy-start.3
  48.0 0.0 copy-done.2
  48.0 0.6 copy-done.4
  48.6 0.0 copy-done.5
  48.6 0.0 copy-done.6
  48.7 0.0 copy-done.3
  48.7 0.8 copy.23.par_ref
  49.5 0.0 copy-start
  49.5 0.0 copy-start.1
  49.5 6.7 %mix.1.a_ref = bf16[80,1024]{1,0:T(8,128)(2,1)} custom-call(bf16[128,1024]{1,0:T(8,128)(2,1)} %get-tuple-element.8.p_ref, bf16[4,64,1024]{2,1,0:T(8,128)(2,1)} %get-tuple-element.9.qf_ref, f32[8,8,128]{2,1,0:T(8,128)} %get-tuple-element.10.jump_ref, f32[256,35]{1,0:T(8,128)} %copy.23.par_ref), custom_call_target="tpu_custom_call" | custom-call | tf_op jit(solution)/shard_map/mix/pallas_call | solution.py:676
  56.2 0.0 copy-done
  56.2 0.0 copy-done.1
  56.2 0.7 pad_maximum_fusion.wo_ref
  56.9 43.8 %output.1 = bf16[32,2048]{1,0:T(8,128)(2,1)} custom-call(bf16[80,1024]{1,0:T(8,128)(2,1)} %mix.1.a_ref, bf16[512,256]{1,0:T(8,128)(2,1)} %pad_maximum_fusion.wo_ref, f32[256,35]{1,0:T(8,128)} %copy.23.par_ref), custom_call_target="tpu_custom_call" | custom-call | tf_op jit(solution)/shard_map/output/pallas_call | solution.py:685
  100.7 1.6 %copy.26 = bf16[32,2048]{1,0:T(8,128)(2,1)} copy(bf16[32,2048]{1,0:T(8,128)(2,1)} %output.1) | data formatting | bytes 262144
  (1 shorter events, 0.0 us)
Async XLA Ops:
  1.3 46.7 %copy-start.2 = (f32[31,256]{1,0:T(8,128)S(1)}, f32[31,256]{1,0:T(8,128)}, u32[]{:S(2)}) copy-start(f32[31,256]{1,0:T(8,128)} %param.20) | copy-start | bytes 95236
  47.9 0.7 copy-start.4
  48.0 0.7 copy-start.5
  48.0 0.7 copy-start.6
  48.0 0.7 copy-start.3
  49.5 6.7 %copy-start = (bf16[256,256]{1,0:T(8,128)(2,1)S(1)}, bf16[256,256]{1,0:T(8,128)(2,1)}, u32[]{:S(2)}) copy-start(bf16[256,256]{1,0:T(8,128)(2,1)} %param.31) | copy-start | bytes 393220
  49.5 6.7 %copy-start.1 = (bf16[256,256]{1,0:T(8,128)(2,1)S(1)}, bf16[256,256]{1,0:T(8,128)(2,1)}, u32[]{:S(2)}) copy-start(bf16[256,256]{1,0:T(8,128)(2,1)} %param.30) | copy-start | bytes 393220

commit v3 on v2

--- a/solution.py
+++ b/solution.py
@@ -255,11 +255,11 @@
 
 
 def project_kernel(
-    sizes, x_hbm, gain_ref, j_ref, cv, cg, rv, og, qw, fw, p_ref, qf_ref, jump_ref,
+    sizes, x_hbm, gain_ref, j_ref, cv, cg, rv, og, qw, fw, co, ro, p_ref, qf_ref, jump_ref, wo_ref,
     x_ref, raw, w_ref, held, weights, load, *sems
 ):
     n_sp, n_tp, rows, depth, chans, members = sizes
-    (send_z, send_x, send_y, send_c, lane, sib, send_w, recv_w, send_j, recv_j, send_q, recv_q) = sems
+    (send_z, send_x, send_y, send_c, lane, sib, send_w, recv_w, send_j, recv_j, send_q, recv_q, swap) = sems
     s, t = lax.axis_index("sp"), lax.axis_index("tp")
     n_z = n_sp // STRIDE
     z, x = s // STRIDE, s % STRIDE
@@ -291,6 +291,11 @@
     loads = [pltpu.make_async_copy(x_hbm, x_ref, load.at[0])] + [
         pltpu.make_async_copy(w, raw.at[i], load.at[1 + i]) for i, w in enumerate(kinds)
     ]
+    cols = co.shape[1]
+    swapped = wo_ref.at[:, pl.ds(pl.multiple_of(z % 2 * cols, cols), cols)]
+    for i, w in enumerate((co, ro)):
+        tall = w.shape[0]
+        loads.append(pltpu.make_async_copy(w, swapped.at[i * tall : (i + 1) * tall, :], load.at[1 + len(kinds) + i]))
     for copy in loads:
         copy.start()
     own = slot(0, 0, 0, c)
@@ -341,6 +346,10 @@
     for dz in near_first:
         send_weights(0, dz)
     weights[:, my_columns] = w_ref[s]
+    for copy in loads[1 + len(kinds) :]:
+        copy.wait()
+    partner = at((z + 1 - z % 2 * 2) * STRIDE + x, t)
+    launch(remote(swapped, swapped, swap.at[0], swap.at[1], partner))
 
     def arrived(dy, dx, dz):
         here = held.at[slot(dy, dx, dz, c)]
@@ -401,6 +410,8 @@
     for k in range(1, n_sp):
         there = jump_ref.at[lax.rem(s - k + n_sp, n_sp)]
         remote(there, there, send_j.at[k], recv_j.at[k], c_peer).wait_recv()
+    other = wo_ref.at[:, pl.ds(pl.multiple_of((1 - z % 2) * cols, cols), cols)]
+    remote(other, other, swap.at[0], swap.at[1], c_peer).wait_recv()
     for copy in pending:
         copy.wait_send()
 
@@ -437,7 +448,15 @@
     for back in range(1, width):
         moved = jnp.where(place >= back, pltpu.roll(gated, back, 1), 0.0)
         conv = conv + moved * mine[:, width - 1 - back : width - back]
-    a_ref[0:chans, :] = conv.astype(bf16)
+
+    def put(start, stop, array):
+        for b in range(n_sp):
+            place = (b // (2 * STRIDE)) * STRIDE + b % STRIDE
+            a_ref[(b // STRIDE) % 2, start:stop, place * part : (place + 1) * part] = array[
+                :, b * part : (b + 1) * part
+            ]
+
+    put(0, chans, conv.astype(bf16))
 
     picked = lax.broadcasted_iota(jnp.int32, jump_ref.shape[1:], 0) == head
     arranged = [in_order(qf_ref[m].astype(f32), n_sp) for m in range(members)]
@@ -482,14 +501,19 @@
     rec = r_s[...].T
     outgate = projected[3 * chans : 4 * chans]
     square = jnp.sum(rec * rec, axis=0, keepdims=True)
-    a_ref[chans : 2 * chans, :] = (
-        rec * mine[:, width : width + 1] * (outgate * jax.nn.sigmoid(outgate))
-    ).astype(bf16)
+    put(
+        chans,
+        2 * chans,
+        (rec * mine[:, width : width + 1] * (outgate * jax.nn.sigmoid(outgate))).astype(bf16),
+    )
     upper = square.astype(bf16).astype(f32)
-    line = lax.broadcasted_iota(jnp.int32, (a_ref.shape[0] - 2 * chans, total), 0)
-    a_ref[2 * chans :, :] = jnp.where(
-        line == 0, upper, jnp.where(line == 1, square - upper, 0.0)
-    ).astype(bf16)
+    tall = a_ref.shape[1]
+    line = lax.broadcasted_iota(jnp.int32, (tall - 2 * chans, total), 0)
+    put(
+        2 * chans,
+        tall,
+        jnp.where(line == 0, upper, jnp.where(line == 1, square - upper, 0.0)).astype(bf16),
+    )
 
 
 def output_kernel(
@@ -501,6 +525,7 @@
     s, t = lax.axis_index("sp"), lax.axis_index("tp")
     n_z = n_sp // STRIDE
     z, x = s // STRIDE, s % STRIDE
+    parity = z % 2
     x_peer = at(z * STRIDE + (1 - x), t)
 
     def sp_at(k):
@@ -516,21 +541,23 @@
         copy.start()
         pending.append(copy)
 
-    for k in range(1, n_z):
-        peer = at(lax.rem(z + k, n_z) * STRIDE + x, t)
-        launch(remote(a_ref, held.at[s], send_z.at[k], recv_z.at[k], peer))
-    launch(remote(a_ref, held.at[s], send_x.at[0], recv_x.at[0], x_peer))
-    held[s] = a_ref[...]
-    for k in range(1, n_z):
-        source = lax.rem(z - k + n_z, n_z) * STRIDE + x
-        here = held.at[source]
+    near_first = sorted(range(1, n_z), key=lambda k: min(k, n_z - k))
+    for k in near_first:
+        z_to = lax.rem(z + k, n_z)
+        launch(
+            remote(a_ref.at[z_to % 2], held.at[s], send_z.at[k], recv_z.at[k], at(z_to * STRIDE + x, t))
+        )
+    launch(remote(a_ref.at[parity], held.at[s], send_x.at[0], recv_x.at[0], x_peer))
+    held[s] = a_ref[parity]
+    for k in near_first:
+        here = held.at[lax.rem(z - k + n_z, n_z) * STRIDE + x]
         remote(here, here, send_z.at[k], recv_z.at[k], x_peer).wait_recv()
         launch(remote(here, here, send_x.at[k], recv_x.at[k], x_peer))
-    for k in range(n_z):
+    for k in [0] + near_first:
         here = held.at[lax.rem(z - k + n_z, n_z) * STRIDE + (1 - x)]
         remote(here, here, send_x.at[k], recv_x.at[k], x_peer).wait_recv()
 
-    total = a_ref.shape[1]
+    total = a_ref.shape[2]
     conv = held[:, 0:chans, :].reshape(n_sp * chans, total).astype(f32)
     sums[t, 0:1, :] = jnp.sum(conv, axis=0, keepdims=True)
     sums[t, 1:2, :] = jnp.sum(conv * conv, axis=0, keepdims=True)
@@ -542,49 +569,71 @@
     both = sums[0]
     for k in range(1, n_tp):
         both = both + sums[k]
-    mean = both[0:1] / channels
-    scale = lax.rsqrt(both[1:2] / channels - mean * mean + layer_eps)
+    sums[n_tp] = both
     gain = par_ref[:, width + 2 : width + 3]
     bias = par_ref[:, width + 3 : width + 4]
     span = members * chans
     heads = n_sp // members
     step = rows * n_tp
-    for b in range(n_sp):
-        lanes = slice(b * step, (b + 1) * step)
+    blocks = n_sp // 2
+    here = (z // 2) * STRIDE + x
+
+    def device(place):
+        return (place // STRIDE * 2 + parity) * STRIDE + place % STRIDE
+
+    def project_block(r):
+        lanes = pl.ds(pl.multiple_of(lax.rem(here + r, blocks) * step, step), step)
+        mean = sums[n_tp, 0:1, lanes] / channels
+        scale = lax.rsqrt(sums[n_tp, 1:2, lanes] / channels - mean * mean + layer_eps)
         values = held[:, 0:chans, lanes].reshape(n_sp * chans, step).astype(f32)
-        shifted = (values - mean[:, lanes]) * scale[:, lanes] * gain + bias
+        shifted = (values - mean) * scale * gain + bias
         pieces = [(shifted * jax.nn.sigmoid(shifted)).astype(bf16)]
         for h in range(heads):
             group = slice(h * members, (h + 1) * members)
-            square = jnp.sum(held[group, 2 * chans : 2 * chans + 16, lanes].astype(f32), axis=(0, 1), keepdims=True)[0]
+            square = jnp.sum(
+                held[group, 2 * chans : 2 * chans + 16, lanes].astype(f32), axis=(0, 1), keepdims=True
+            )[0]
             ups = held[group, chans : 2 * chans, lanes].reshape(span, step).astype(f32)
             pieces.append((ups * lax.rsqrt(square / span + norm_eps)).astype(bf16))
         out = lax.dot_general(
             jnp.concatenate(pieces, axis=0), wo_ref[...], TN, preferred_element_type=f32
         ).astype(bf16)
         for k in range(n_tp):
-            part[k, b * rows : (b + 1) * rows, :] = out[k * rows : (k + 1) * rows]
-    for k in range(1, n_tp):
-        launch(remote(part.at[tp_at(k)], got.at[k], send_p.at[k], recv_p.at[k], at(s, tp_at(k))))
-    added = part[t].astype(f32)
-    for k in range(1, n_tp):
-        remote(got.at[k], got.at[k], send_p.at[k], recv_p.at[k], x_peer).wait_recv()
-        added = added + got[k].astype(f32)
-    mixed[...] = added.astype(bf16)
-    cols = wo_ref.shape[1]
-
-    def window(source):
-        return o_ref.at[:, pl.ds(pl.multiple_of(source * cols, cols), cols)]
-
-    def block_of(sp):
-        return pl.ds(pl.multiple_of(sp * rows, rows), rows)
-
-    for k in range(1, n_sp):
-        launch(remote(mixed.at[block_of(sp_at(k))], window(s), send_o.at[k], recv_o.at[k], at(sp_at(k), t)))
-    window(s)[...] = mixed[block_of(s), :]
-    for k in range(1, n_sp):
-        there = window(lax.rem(s - k + n_sp, n_sp))
-        remote(there, there, send_o.at[k], recv_o.at[k], x_peer).wait_recv()
+            part[k, r] = out[k * rows : (k + 1) * rows]
+        for k in range(1, n_tp):
+            launch(
+                remote(part.at[tp_at(k), r], got.at[k, r], send_p.at[k, r], recv_p.at[k, r], at(s, tp_at(k)))
+            )
+
+    cols = wo_ref.shape[1] // 2
+
+    def window(place, p):
+        column = (place // STRIDE * 2 + p) * STRIDE + place % STRIDE
+        return o_ref.at[:, pl.ds(pl.multiple_of(column * cols, cols), cols)]
+
+    def finish_block(r):
+        added = part[t, r].astype(f32)
+        for k in range(1, n_tp):
+            remote(got.at[k, r], got.at[k, r], send_p.at[k, r], recv_p.at[k, r], x_peer).wait_recv()
+            added = added + got[k, r].astype(f32)
+        mixed[r] = added.astype(bf16)
+        for p in range(2):
+            piece = mixed.at[r, :, p * cols : (p + 1) * cols]
+            if r:
+                to = at(device(lax.rem(here + r, blocks)), t)
+                launch(remote(piece, window(here, p), send_o.at[r, p], recv_o.at[r, p], to))
+            else:
+                window(here, p)[...] = piece[...]
+
+    order = list(range(1, blocks)) + [0]
+    for r in order:
+        project_block(r)
+    for r in order:
+        finish_block(r)
+    for r in range(1, blocks):
+        for p in range(2):
+            there = window(lax.rem(here - r + blocks, blocks), p)
+            remote(there, there, send_o.at[r, p], recv_o.at[r, p], x_peer).wait_recv()
     for copy in pending:
         copy.wait_send()
 
@@ -633,29 +682,30 @@
         ],
         axis=1,
     )
-    weights_out = jnp.concatenate([convolution_output_weight, recurrence_output_weight], axis=0)
+    cols = convolution_output_weight.shape[1]
     vmem = pl.BlockSpec(memory_space=pltpu.VMEM)
     anywhere = pl.BlockSpec(memory_space=pl.ANY)
     dma = pltpu.SemaphoreType.DMA
     bf16, f32 = jnp.bfloat16, jnp.float32
     n_z = n_sp // STRIDE
     lanes = 2 * n_sp
-    projected, query_forget, all_jumps = pl.pallas_call(
+    projected, query_forget, all_jumps, weights_out = pl.pallas_call(
         functools.partial(project_kernel, (n_sp, n_tp, rows, depth, chans, members)),
         out_shape=(
             jax.ShapeDtypeStruct((4 * chans, total), bf16),
             jax.ShapeDtypeStruct((members, 2 * chans, total), bf16),
             jax.ShapeDtypeStruct((n_sp, *jumps.shape), f32),
+            jax.ShapeDtypeStruct((2 * group_chans, 2 * cols), bf16),
         ),
-        in_specs=[anywhere, vmem, vmem] + [anywhere] * len(kinds),
-        out_specs=(vmem,) * 3,
+        in_specs=[anywhere, vmem, vmem] + [anywhere] * (len(kinds) + 2),
+        out_specs=(vmem,) * 4,
         scratch_shapes=[
             pltpu.VMEM((rows, model), bf16),
             pltpu.VMEM((len(kinds), depth, group_chans), bf16),
             pltpu.VMEM((n_sp, len(kinds) * chans, depth), bf16),
             pltpu.VMEM((total, model), bf16),
             pltpu.VMEM((len(kinds) * chans, model), bf16),
-            dma((1 + len(kinds),)),
+            dma((3 + len(kinds),)),
             dma((n_z,)),
             dma((n_z,)),
             dma((lanes,)),
@@ -668,20 +718,27 @@
             dma((n_sp,)),
             dma((2, members)),
             dma((2, members)),
+            dma((2,)),
         ],
         compiler_params=pltpu.CompilerParams(collective_id=0, has_side_effects=True),
         name="project",
-    )(tokens, input_norm_gain[None, :], jumps, *kinds)
+    )(
+        tokens,
+        input_norm_gain[None, :],
+        jumps,
+        *kinds,
+        convolution_output_weight,
+        recurrence_output_weight,
+    )
     span = members * chans
     sent = pl.pallas_call(
         functools.partial(mix_kernel, (n_sp, chans, members, width, HG_BLOCK, part)),
-        out_shape=jax.ShapeDtypeStruct((2 * chans + 16, total), bf16),
+        out_shape=jax.ShapeDtypeStruct((2, 2 * chans + 16, total // 2), bf16),
         in_specs=[vmem] * 4,
         out_specs=vmem,
         scratch_shapes=[pltpu.VMEM((total, span), f32)] * 3 + [pltpu.VMEM((total, chans), f32)],
         name="mix",
     )(projected, query_forget, all_jumps, params)
-    cols = weights_out.shape[1]
     return pl.pallas_call(
         functools.partial(
             output_kernel, (n_sp, n_tp, rows, chans, members, width, group_chans * n_tp)
@@ -690,21 +747,21 @@
         in_specs=[vmem] * 3,
         out_specs=vmem,
         scratch_shapes=[
-            pltpu.VMEM((n_sp, 2 * chans + 16, total), bf16),
-            pltpu.VMEM((n_tp, 8, total), f32),
-            pltpu.VMEM((n_tp, n_sp * rows, cols), bf16),
-            pltpu.VMEM((n_tp, n_sp * rows, cols), bf16),
-            pltpu.VMEM((n_sp * rows, cols), bf16),
+            pltpu.VMEM((n_sp, 2 * chans + 16, total // 2), bf16),
+            pltpu.VMEM((n_tp + 1, 8, total // 2), f32),
+            pltpu.VMEM((n_tp, n_sp // 2, rows, 2 * cols), bf16),
+            pltpu.VMEM((n_tp, n_sp // 2, rows, 2 * cols), bf16),
+            pltpu.VMEM((n_sp // 2, rows, 2 * cols), bf16),
             dma((n_z,)),
             dma((n_z,)),
             dma((n_z,)),
             dma((n_z,)),
             dma((n_tp,)),
             dma((n_tp,)),
-            dma((n_tp,)),
-            dma((n_tp,)),
-            dma((n_sp,)),
-            dma((n_sp,)),
+            dma((n_tp, n_sp // 2)),
+            dma((n_tp, n_sp // 2)),
+            dma((n_sp // 2, 2)),
+            dma((n_sp // 2, 2)),
         ],
         compiler_params=pltpu.CompilerParams(collective_id=1, has_side_effects=True),
         name="output",
@@ -717,7 +774,7 @@
     heads = arrays[12].shape[0]
     gathered_bytes = rows * n_sp * n_tp * model * arrays[0].dtype.itemsize
     fits = gathered_bytes <= 2**23
-    even = n_tp == 4 and n_sp % heads == 0 and n_sp % STRIDE == 0 and group_chans % (32 * n_sp) == 0
+    even = n_tp == 4 and n_sp % heads == 0 and n_sp % (2 * STRIDE) == 0 and group_chans % (32 * n_sp) == 0
     if fits and even:
         return spread_channels(n_sp, n_tp, *arrays)
     return per_device(*arrays)

time: 104 us -> 89.4 us (0.86); the launches traced: 102 us -> 88.9 us
  Pallas kernels: 97.1 us -> 84.3 us
    pallas_call x1, Pallas kernels: 43.8 us -> 30.9 us  [spread_channels(): pl.pallas_call(functools.partial(output_kernel, (n_sp, n_tp, rows, chans,...]
    unnamed x15 -> x11, local copies, waits for them, and re-layouts: 2.27 us -> 2.37 us
where the time goes in v3:
time: 89.4 us; the launch traced here: 88.9 us
  Pallas kernels  84.3 us (94%)
  local copies, waits for them, and re-layouts  4.54 us (5%)
    pallas_call x1, Pallas kernels, spread_channels(): pl.pallas_call(functools.partial(project_kernel, (n_sp, n_tp, rows, depth...  46.7 us
    pallas_call x1, Pallas kernels, spread_channels(): pl.pallas_call(functools.partial(output_kernel, (n_sp, n_tp, rows, chans,...  30.9 us
    pallas_call x1, Pallas kernels, spread_channels(): pl.pallas_call(functools.partial(mix_kernel, (n_sp, chans, members, width...  6.68 us
    unnamed x11, local copies, waits for them, and re-layouts  2.37 us

profile of v3, /device:TPU:0, one launch (start us, length us, event | category | flops | bytes accessed | tf_op | source)
XLA Modules:
  0.0 88.9 jit_solution(5065192156975002590)
XLA Ops:
  0.0 0.0 copy-start.4
  0.0 0.7 copy-done.4
  0.7 0.0 copy-start
  0.7 0.0 copy-start.1
  0.7 0.0 copy-start.2
  0.7 0.0 copy-start.3
  0.7 0.6 pad.4.j_ref
  1.3 0.1 copy-done
  1.4 0.0 copy-done.1
  1.4 0.0 copy-done.2
  1.4 0.0 copy-done.3
  1.4 0.8 concatenate.3
  2.2 0.8 copy.23.par_ref
  3.0 46.7 %project.1 = (bf16[128,1024]{1,0:T(8,128)(2,1)}, bf16[4,64,1024]{2,1,0:T(8,128)(2,1)}, f32[8,8,128]{2,1,0:T(8,128)}, bf16[512,512]{1,0:T(8,128)(2,1)}) custom-call(bf16[32,2048]{1,0:T(8,128)(2,1)} %x_hbm.1, f32[1,2048]{1,0:T(1,128)} %bitcast.7, f32[8,128]{1,0:T(8,128)} %pad.4.j_ref, bf16[256,256]{1,0:T(8,128)(2,1)} %cv.1, bf16[256,256]{1,0:T(8,128)(2,1)} %cg.1, ...), custom_call_target="tpu_custom_call" | custom-call | tf_op jit(solution)/shard_map/project/pallas_call | solution.py:692
  49.7 6.7 %mix.1.a_ref = bf16[2,80,512]{2,1,0:T(8,128)(2,1)} custom-call(bf16[128,1024]{1,0:T(8,128)(2,1)} %get-tuple-element.9.p_ref, bf16[4,64,1024]{2,1,0:T(8,128)(2,1)} %get-tuple-element.10.qf_ref, f32[8,8,128]{2,1,0:T(8,128)} %get-tuple-element.11.jump_ref, f32[256,35]{1,0:T(8,128)} %copy.23.par_ref), custom_call_target="tpu_custom_call" | custom-call | tf_op jit(solution)/shard_map/mix/pallas_call | solution.py:734
  56.4 30.9 %output.1 = bf16[32,2048]{1,0:T(8,128)(2,1)} custom-call(bf16[2,80,512]{2,1,0:T(8,128)(2,1)} %mix.1.a_ref, bf16[512,512]{1,0:T(8,128)(2,1)} %get-tuple-element.12.wo_ref, f32[256,35]{1,0:T(8,128)} %copy.23.par_ref), custom_call_target="tpu_custom_call" | custom-call | tf_op jit(solution)/shard_map/output/pallas_call | solution.py:742
  87.3 1.6 %copy.26 = bf16[32,2048]{1,0:T(8,128)(2,1)} copy(bf16[32,2048]{1,0:T(8,128)(2,1)} %output.1) | data formatting | bytes 262144
Async XLA Ops:
  0.0 0.7 copy-start.4
  0.7 0.7 copy-start
  0.7 0.7 copy-start.1
  0.7 0.7 copy-start.2
  0.7 0.7 copy-start.3

commit v4 on v3

--- a/solution.py
+++ b/solution.py
@@ -254,11 +254,14 @@
     )
 
 
-def project_kernel(
-    sizes, x_hbm, gain_ref, j_ref, cv, cg, rv, og, qw, fw, co, ro, p_ref, qf_ref, jump_ref, wo_ref,
-    x_ref, raw, w_ref, held, weights, load, *sems
+def layer_kernel(
+    sizes, x_hbm, gain_ref, j_ref, taps, head_gain, floor, norm_gain, norm_bias,
+    cv, cg, rv, og, qw, fw, co, ro, o_ref, p_ref, qf_ref, jump_ref, wo_ref,
+    x_ref, raw, w_ref, held, weights, par_ref, ac_ref, ar_ref, q_s, k_s, d_s, r_s,
+    conv_all, rec_all, sums, partial, got, mixed, load, *sems
 ):
-    n_sp, n_tp, rows, depth, chans, members = sizes
+    n_sp, n_tp, rows, depth, chans, members, width, block, channels = sizes
+    sems, after = sems[:13], sems[13:]
     (send_z, send_x, send_y, send_c, lane, sib, send_w, recv_w, send_j, recv_j, send_q, recv_q, swap) = sems
     s, t = lax.axis_index("sp"), lax.axis_index("tp")
     n_z = n_sp // STRIDE
@@ -283,7 +286,8 @@
     def number(dy, dx, dz):
         return (dy * STRIDE + dx) * n_z + dz
 
-    peers = [at(sp_peer(k), t) for k in range(1, n_sp)] + [y_peer, c_peer]
+    peers = [at(sp_peer(k), t) for k in range(1, n_sp)]
+    peers += [at(s, lax.rem(t + k, n_tp)) for k in range(1, n_tp)]
     barrier = pltpu.get_barrier_semaphore()
     for peer in peers:
         pl.semaphore_signal(barrier, inc=1, device_id=peer, device_id_type=MESH)
@@ -331,6 +335,10 @@
     for k in range(1, n_sp):
         launch(remote(j_ref, jump_ref.at[s], send_j.at[k], recv_j.at[k], at(sp_peer(k), t)))
     jump_ref[s] = j_ref[...]
+    small = [taps, head_gain, floor, norm_gain, norm_bias]
+    tall = sum(v.shape[0] for v in small)
+    filler = jnp.zeros((-tall % 8, taps.shape[1]), jnp.float32)
+    par_ref[...] = jnp.concatenate([v[...] for v in small] + [filler], axis=0).T
     for i in range(len(kinds)):
         loads[1 + i].wait()
         turned = raw[i].T
@@ -345,6 +353,8 @@
 
     for dz in near_first:
         send_weights(0, dz)
+    for dz in [0] + near_first:
+        send_weights(1, dz)
     weights[:, my_columns] = w_ref[s]
     for copy in loads[1 + len(kinds) :]:
         copy.wait()
@@ -362,8 +372,6 @@
     order.append((1, near_first[-1]))
     for dx, dz in order:
         arrived(0, dx, dz)
-    for dz in [0] + near_first:
-        send_weights(1, dz)
     across = [(0, 0)] + order
     early = len(across) // 2 + 1
     for dx, dz in across[:early]:
@@ -402,6 +410,32 @@
     for dx, dz in across[early:]:
         arrived(1, dx, dz)
     project_half(1)
+    f32, bf16 = jnp.float32, jnp.bfloat16
+    own_params = par_ref[pl.ds(pl.multiple_of(s * chans, chans), chans), :]
+    projected = in_order(p_ref[...].astype(f32), n_sp)
+    convolve_lanes(projected, own_params, ac_ref, sizes)
+    (sc_z, sc_x, rc_z, rc_x, sr_z, sr_x, rr_z, rr_x, send_s, recv_s, send_p, recv_p, send_o, recv_o) = after
+    parity = z % 2
+
+    def spread(src, dst, sz, sx, rz, rx):
+        for k in near_first:
+            z_to = lax.rem(z + k, n_z)
+            launch(remote(src.at[z_to % 2], dst.at[s], sz.at[k], rz.at[k], at(z_to * STRIDE + x, t)))
+        launch(remote(src.at[parity], dst.at[s], sx.at[0], rx.at[0], x_peer))
+        dst[s] = src[parity]
+
+    def forward(dst, sz, sx, rz, rx):
+        for k in near_first:
+            here = dst.at[lax.rem(z - k + n_z, n_z) * STRIDE + x]
+            remote(here, here, sz.at[k], rz.at[k], x_peer).wait_recv()
+            launch(remote(here, here, sx.at[k], rx.at[k], x_peer))
+
+    def collect(dst, sx, rx):
+        for k in [0] + near_first:
+            here = dst.at[lax.rem(z - k + n_z, n_z) * STRIDE + (1 - x)]
+            remote(here, here, sx.at[k], rx.at[k], x_peer).wait_recv()
+
+    spread(ac_ref, conv_all, sc_z, sc_x, rc_z, rc_x)
     for dy in range(2):
         window = pl.ds(pl.multiple_of(((1 - y) if dy else y) * half, half), half)
         for k in range(1, members):
@@ -410,8 +444,93 @@
     for k in range(1, n_sp):
         there = jump_ref.at[lax.rem(s - k + n_sp, n_sp)]
         remote(there, there, send_j.at[k], recv_j.at[k], c_peer).wait_recv()
+    recur(s, projected, own_params, qf_ref, jump_ref, par_ref, ar_ref, q_s, k_s, d_s, r_s, sizes)
+    spread(ar_ref, rec_all, sr_z, sr_x, rr_z, rr_x)
+    forward(conv_all, sc_z, sc_x, rc_z, rc_x)
+    collect(conv_all, sc_x, rc_x)
+    total = ac_ref.shape[2]
+    conv = conv_all[...].reshape(n_sp * chans, total).astype(f32)
+    sums[t, 0:1, :] = jnp.sum(conv, axis=0, keepdims=True)
+    sums[t, 1:2, :] = jnp.sum(conv * conv, axis=0, keepdims=True)
+
+    def tp_at(k):
+        return lax.rem(t + k, n_tp)
+
+    for k in range(1, n_tp):
+        launch(remote(sums.at[t], sums.at[t], send_s.at[k], recv_s.at[k], at(s, tp_at(k))))
+    forward(rec_all, sr_z, sr_x, rr_z, rr_x)
+    for k in range(1, n_tp):
+        there = sums.at[lax.rem(t - k + n_tp, n_tp)]
+        remote(there, there, send_s.at[k], recv_s.at[k], x_peer).wait_recv()
+    collect(rec_all, sr_x, rr_x)
     other = wo_ref.at[:, pl.ds(pl.multiple_of((1 - z % 2) * cols, cols), cols)]
     remote(other, other, swap.at[0], swap.at[1], c_peer).wait_recv()
+    both = sums[0]
+    for k in range(1, n_tp):
+        both = both + sums[k]
+    sums[n_tp] = both
+    gain = par_ref[:, width + 2 : width + 3]
+    bias = par_ref[:, width + 3 : width + 4]
+    span = members * chans
+    heads = n_sp // members
+    step = rows * n_tp
+    blocks = n_sp // 2
+    home = (z // 2) * STRIDE + x
+
+    def device(place):
+        return (place // STRIDE * 2 + parity) * STRIDE + place % STRIDE
+
+    def project_block(r):
+        lanes = pl.ds(pl.multiple_of(lax.rem(home + r, blocks) * step, step), step)
+        mean = sums[n_tp, 0:1, lanes] / channels
+        scale = lax.rsqrt(sums[n_tp, 1:2, lanes] / channels - mean * mean + layer_eps)
+        values = conv_all[:, :, lanes].reshape(n_sp * chans, step).astype(f32)
+        shifted = (values - mean) * scale * gain + bias
+        pieces = [(shifted * jax.nn.sigmoid(shifted)).astype(bf16)]
+        for h in range(heads):
+            group = slice(h * members, (h + 1) * members)
+            square = jnp.sum(
+                rec_all[group, chans:, lanes].astype(f32), axis=(0, 1), keepdims=True
+            )[0]
+            ups = rec_all[group, 0:chans, lanes].reshape(span, step).astype(f32)
+            pieces.append((ups * lax.rsqrt(square / span + norm_eps)).astype(bf16))
+        out = lax.dot_general(
+            jnp.concatenate(pieces, axis=0), wo_ref[...], TN, preferred_element_type=f32
+        ).astype(bf16)
+        for k in range(n_tp):
+            partial[k, r] = out[k * rows : (k + 1) * rows]
+        for k in range(1, n_tp):
+            launch(
+                remote(partial.at[tp_at(k), r], got.at[k, r], send_p.at[k, r], recv_p.at[k, r], at(s, tp_at(k)))
+            )
+
+    def window(place, p):
+        column = (place // STRIDE * 2 + p) * STRIDE + place % STRIDE
+        return o_ref.at[:, pl.ds(pl.multiple_of(column * cols, cols), cols)]
+
+    def finish_block(r):
+        added = partial[t, r].astype(f32)
+        for k in range(1, n_tp):
+            remote(got.at[k, r], got.at[k, r], send_p.at[k, r], recv_p.at[k, r], x_peer).wait_recv()
+            added = added + got[k, r].astype(f32)
+        mixed[r] = added.astype(bf16)
+        for p in range(2):
+            piece = mixed.at[r, :, p * cols : (p + 1) * cols]
+            if r:
+                to = at(device(lax.rem(home + r, blocks)), t)
+                launch(remote(piece, window(home, p), send_o.at[r, p], recv_o.at[r, p], to))
+            else:
+                window(home, p)[...] = piece[...]
+
+    sequence = list(range(1, blocks)) + [0]
+    for r in sequence:
+        project_block(r)
+    for r in sequence:
+        finish_block(r)
+    for r in range(1, blocks):
+        for p in range(2):
+            there = window(lax.rem(home - r + blocks, blocks), p)
+            remote(there, there, send_o.at[r, p], recv_o.at[r, p], x_peer).wait_recv()
     for copy in pending:
         copy.wait_send()
 
@@ -429,17 +548,17 @@
     )
 
 
-def mix_kernel(sizes, p_ref, qf_ref, jump_ref, par_ref, a_ref, q_s, k_s, d_s, r_s):
-    n_sp, chans, members, width, block, part = sizes
-    s = lax.axis_index("sp")
-    total = p_ref.shape[1]
-    f32, bf16 = jnp.float32, jnp.bfloat16
-    mine = par_ref[pl.ds(pl.multiple_of(s * chans, chans), chans), :]
-    head = s // members
-    span = chans * members
-    margin = par_ref[pl.ds(pl.multiple_of(head * span, span), span), width + 1 : width + 2]
-
-    projected = in_order(p_ref[...].astype(f32), n_sp)
+def put(ref, n_sp, start, stop, array):
+    part = array.shape[1] // n_sp
+    for b in range(n_sp):
+        place = (b // (2 * STRIDE)) * STRIDE + b % STRIDE
+        ref[(b // STRIDE) % 2, start:stop, place * part : (place + 1) * part] = array[
+            :, b * part : (b + 1) * part
+        ]
+
+
+def convolve_lanes(projected, mine, ac_ref, sizes):
+    n_sp, chans, width = sizes[0], sizes[4], sizes[6]
     value = projected[0:chans]
     gate = projected[chans : 2 * chans]
     gated = value * jax.nn.sigmoid(gate)
@@ -448,16 +567,17 @@
     for back in range(1, width):
         moved = jnp.where(place >= back, pltpu.roll(gated, back, 1), 0.0)
         conv = conv + moved * mine[:, width - 1 - back : width - back]
-
-    def put(start, stop, array):
-        for b in range(n_sp):
-            place = (b // (2 * STRIDE)) * STRIDE + b % STRIDE
-            a_ref[(b // STRIDE) % 2, start:stop, place * part : (place + 1) * part] = array[
-                :, b * part : (b + 1) * part
-            ]
-
-    put(0, chans, conv.astype(bf16))
-
+    put(ac_ref, n_sp, 0, chans, conv.astype(jnp.bfloat16))
+
+
+def recur(s, projected, mine, qf_ref, jump_ref, par_ref, ar_ref, q_s, k_s, d_s, r_s, sizes):
+    n_sp, n_tp, rows, depth, chans, members, width, block, channels = sizes
+    total = projected.shape[1]
+    part = total // n_sp
+    f32, bf16 = jnp.float32, jnp.bfloat16
+    head = s // members
+    span = chans * members
+    margin = par_ref[pl.ds(pl.multiple_of(head * span, span), span), width + 1 : width + 2]
     picked = lax.broadcasted_iota(jnp.int32, jump_ref.shape[1:], 0) == head
     arranged = [in_order(qf_ref[m].astype(f32), n_sp) for m in range(members)]
     for b in range(n_sp):
@@ -502,140 +622,22 @@
     outgate = projected[3 * chans : 4 * chans]
     square = jnp.sum(rec * rec, axis=0, keepdims=True)
     put(
+        ar_ref,
+        n_sp,
+        0,
         chans,
-        2 * chans,
         (rec * mine[:, width : width + 1] * (outgate * jax.nn.sigmoid(outgate))).astype(bf16),
     )
     upper = square.astype(bf16).astype(f32)
-    tall = a_ref.shape[1]
-    line = lax.broadcasted_iota(jnp.int32, (tall - 2 * chans, total), 0)
+    tall = ar_ref.shape[1]
+    line = lax.broadcasted_iota(jnp.int32, (tall - chans, total), 0)
     put(
-        2 * chans,
+        ar_ref,
+        n_sp,
+        chans,
         tall,
         jnp.where(line == 0, upper, jnp.where(line == 1, square - upper, 0.0)).astype(bf16),
     )
-
-
-def output_kernel(
-    sizes, a_ref, wo_ref, par_ref, o_ref, held, sums, part, got, mixed, *sems
-):
-    n_sp, n_tp, rows, chans, members, width, channels = sizes
-    send_z, send_x, recv_z, recv_x, send_s, recv_s, send_p, recv_p, send_o, recv_o = sems
-    f32, bf16 = jnp.float32, jnp.bfloat16
-    s, t = lax.axis_index("sp"), lax.axis_index("tp")
-    n_z = n_sp // STRIDE
-    z, x = s // STRIDE, s % STRIDE
-    parity = z % 2
-    x_peer = at(z * STRIDE + (1 - x), t)
-
-    def sp_at(k):
-        return lax.rem(s + k, n_sp)
-
-    def tp_at(k):
-        return lax.rem(t + k, n_tp)
-
-    greet([at(sp_at(k), t) for k in range(1, n_sp)] + [at(s, tp_at(k)) for k in range(1, n_tp)])
-    pending = []
-
-    def launch(copy):
-        copy.start()
-        pending.append(copy)
-
-    near_first = sorted(range(1, n_z), key=lambda k: min(k, n_z - k))
-    for k in near_first:
-        z_to = lax.rem(z + k, n_z)
-        launch(
-            remote(a_ref.at[z_to % 2], held.at[s], send_z.at[k], recv_z.at[k], at(z_to * STRIDE + x, t))
-        )
-    launch(remote(a_ref.at[parity], held.at[s], send_x.at[0], recv_x.at[0], x_peer))
-    held[s] = a_ref[parity]
-    for k in near_first:
-        here = held.at[lax.rem(z - k + n_z, n_z) * STRIDE + x]
-        remote(here, here, send_z.at[k], recv_z.at[k], x_peer).wait_recv()
-        launch(remote(here, here, send_x.at[k], recv_x.at[k], x_peer))
-    for k in [0] + near_first:
-        here = held.at[lax.rem(z - k + n_z, n_z) * STRIDE + (1 - x)]
-        remote(here, here, send_x.at[k], recv_x.at[k], x_peer).wait_recv()
-
-    total = a_ref.shape[2]
-    conv = held[:, 0:chans, :].reshape(n_sp * chans, total).astype(f32)
-    sums[t, 0:1, :] = jnp.sum(conv, axis=0, keepdims=True)
-    sums[t, 1:2, :] = jnp.sum(conv * conv, axis=0, keepdims=True)
-    for k in range(1, n_tp):
-        launch(remote(sums.at[t], sums.at[t], send_s.at[k], recv_s.at[k], at(s, tp_at(k))))
-    for k in range(1, n_tp):
-        there = sums.at[lax.rem(t - k + n_tp, n_tp)]
-        remote(there, there, send_s.at[k], recv_s.at[k], x_peer).wait_recv()
-    both = sums[0]
-    for k in range(1, n_tp):
-        both = both + sums[k]
-    sums[n_tp] = both
-    gain = par_ref[:, width + 2 : width + 3]
-    bias = par_ref[:, width + 3 : width + 4]
-    span = members * chans
-    heads = n_sp // members
-    step = rows * n_tp
-    blocks = n_sp // 2
-    here = (z // 2) * STRIDE + x
-
-    def device(place):
-        return (place // STRIDE * 2 + parity) * STRIDE + place % STRIDE
-
-    def project_block(r):
-        lanes = pl.ds(pl.multiple_of(lax.rem(here + r, blocks) * step, step), step)
-        mean = sums[n_tp, 0:1, lanes] / channels
-        scale = lax.rsqrt(sums[n_tp, 1:2, lanes] / channels - mean * mean + layer_eps)
-        values = held[:, 0:chans, lanes].reshape(n_sp * chans, step).astype(f32)
-        shifted = (values - mean) * scale * gain + bias
-        pieces = [(shifted * jax.nn.sigmoid(shifted)).astype(bf16)]
-        for h in range(heads):
-            group = slice(h * members, (h + 1) * members)
-            square = jnp.sum(
-                held[group, 2 * chans : 2 * chans + 16, lanes].astype(f32), axis=(0, 1), keepdims=True
-            )[0]
-            ups = held[group, chans : 2 * chans, lanes].reshape(span, step).astype(f32)
-            pieces.append((ups * lax.rsqrt(square / span + norm_eps)).astype(bf16))
-        out = lax.dot_general(
-            jnp.concatenate(pieces, axis=0), wo_ref[...], TN, preferred_element_type=f32
-        ).astype(bf16)
-        for k in range(n_tp):
-            part[k, r] = out[k * rows : (k + 1) * rows]
-        for k in range(1, n_tp):
-            launch(
-                remote(part.at[tp_at(k), r], got.at[k, r], send_p.at[k, r], recv_p.at[k, r], at(s, tp_at(k)))
-            )
-
-    cols = wo_ref.shape[1] // 2
-
-    def window(place, p):
-        column = (place // STRIDE * 2 + p) * STRIDE + place % STRIDE
-        return o_ref.at[:, pl.ds(pl.multiple_of(column * cols, cols), cols)]
-
-    def finish_block(r):
-        added = part[t, r].astype(f32)
-        for k in range(1, n_tp):
-            remote(got.at[k, r], got.at[k, r], send_p.at[k, r], recv_p.at[k, r], x_peer).wait_recv()
-            added = added + got[k, r].astype(f32)
-        mixed[r] = added.astype(bf16)
-        for p in range(2):
-            piece = mixed.at[r, :, p * cols : (p + 1) * cols]
-            if r:
-                to = at(device(lax.rem(here + r, blocks)), t)
-                launch(remote(piece, window(here, p), send_o.at[r, p], recv_o.at[r, p], to))
-            else:
-                window(here, p)[...] = piece[...]
-
-    order = list(range(1, blocks)) + [0]
-    for r in order:
-        project_block(r)
-    for r in order:
-        finish_block(r)
-    for r in range(1, blocks):
-        for p in range(2):
-            there = window(lax.rem(here - r + blocks, blocks), p)
-            remote(there, there, send_o.at[r, p], recv_o.at[r, p], x_peer).wait_recv()
-    for copy in pending:
-        copy.wait_send()
 
 
 def spread_channels(n_sp, n_tp,
@@ -671,17 +673,6 @@
         query_projection_weight,
         forget_gate_weight,
     )
-    jumps = jnp.pad(decay_jump_terms, ((0, -heads % 8), (0, 0)))
-    params = jnp.concatenate(
-        [
-            depthwise_filter_taps.T,
-            head_norm_gain[:, None],
-            forget_floor_margin[:, None],
-            channel_norm_gain[:, None],
-            channel_norm_bias[:, None],
-        ],
-        axis=1,
-    )
     cols = convolution_output_weight.shape[1]
     vmem = pl.BlockSpec(memory_space=pltpu.VMEM)
     anywhere = pl.BlockSpec(memory_space=pl.ANY)
@@ -689,22 +680,41 @@
     bf16, f32 = jnp.bfloat16, jnp.float32
     n_z = n_sp // STRIDE
     lanes = 2 * n_sp
-    projected, query_forget, all_jumps, weights_out = pl.pallas_call(
-        functools.partial(project_kernel, (n_sp, n_tp, rows, depth, chans, members)),
-        out_shape=(
-            jax.ShapeDtypeStruct((4 * chans, total), bf16),
-            jax.ShapeDtypeStruct((members, 2 * chans, total), bf16),
-            jax.ShapeDtypeStruct((n_sp, *jumps.shape), f32),
-            jax.ShapeDtypeStruct((2 * group_chans, 2 * cols), bf16),
+    span = members * chans
+    blocks = n_sp // 2
+    sums_rows = 16
+    n_params = width + 4 + -(width + 4) % 8
+    return pl.pallas_call(
+        functools.partial(
+            layer_kernel,
+            (n_sp, n_tp, rows, depth, chans, members, width, HG_BLOCK, group_chans * n_tp),
         ),
-        in_specs=[anywhere, vmem, vmem] + [anywhere] * (len(kinds) + 2),
-        out_specs=(vmem,) * 4,
+        out_shape=jax.ShapeDtypeStruct((rows, model), bf16),
+        in_specs=[anywhere] + [vmem] * 7 + [anywhere] * (len(kinds) + 2),
+        out_specs=vmem,
         scratch_shapes=[
+            pltpu.VMEM((4 * chans, total), bf16),
+            pltpu.VMEM((members, 2 * chans, total), bf16),
+            pltpu.VMEM((n_sp, *decay_jump_terms.shape), f32),
+            pltpu.VMEM((2 * group_chans, 2 * cols), bf16),
             pltpu.VMEM((rows, model), bf16),
             pltpu.VMEM((len(kinds), depth, group_chans), bf16),
             pltpu.VMEM((n_sp, len(kinds) * chans, depth), bf16),
             pltpu.VMEM((total, model), bf16),
             pltpu.VMEM((len(kinds) * chans, model), bf16),
+            pltpu.VMEM((group_chans, n_params), f32),
+            pltpu.VMEM((2, chans, total // 2), bf16),
+            pltpu.VMEM((2, chans + sums_rows, total // 2), bf16),
+            pltpu.VMEM((total, span), f32),
+            pltpu.VMEM((total, span), f32),
+            pltpu.VMEM((total, span), f32),
+            pltpu.VMEM((total, chans), f32),
+            pltpu.VMEM((n_sp, chans, total // 2), bf16),
+            pltpu.VMEM((n_sp, chans + sums_rows, total // 2), bf16),
+            pltpu.VMEM((n_tp + 1, 8, total // 2), f32),
+            pltpu.VMEM((n_tp, blocks, rows, 2 * cols), bf16),
+            pltpu.VMEM((n_tp, blocks, rows, 2 * cols), bf16),
+            pltpu.VMEM((blocks, rows, 2 * cols), bf16),
             dma((3 + len(kinds),)),
             dma((n_z,)),
             dma((n_z,)),
@@ -719,53 +729,31 @@
             dma((2, members)),
             dma((2, members)),
             dma((2,)),
+        ]
+        + [dma((n_z,))] * 8
+        + [
+            dma((n_tp,)),
+            dma((n_tp,)),
+            dma((n_tp, blocks)),
+            dma((n_tp, blocks)),
+            dma((blocks, 2)),
+            dma((blocks, 2)),
         ],
         compiler_params=pltpu.CompilerParams(collective_id=0, has_side_effects=True),
-        name="project",
+        name="layer",
     )(
         tokens,
         input_norm_gain[None, :],
-        jumps,
+        decay_jump_terms,
+        depthwise_filter_taps,
+        head_norm_gain[None, :],
+        forget_floor_margin[None, :],
+        channel_norm_gain[None, :],
+        channel_norm_bias[None, :],
         *kinds,
         convolution_output_weight,
         recurrence_output_weight,
     )
-    span = members * chans
-    sent = pl.pallas_call(
-        functools.partial(mix_kernel, (n_sp, chans, members, width, HG_BLOCK, part)),
-        out_shape=jax.ShapeDtypeStruct((2, 2 * chans + 16, total // 2), bf16),
-        in_specs=[vmem] * 4,
-        out_specs=vmem,
-        scratch_shapes=[pltpu.VMEM((total, span), f32)] * 3 + [pltpu.VMEM((total, chans), f32)],
-        name="mix",
-    )(projected, query_forget, all_jumps, params)
-    return pl.pallas_call(
-        functools.partial(
-            output_kernel, (n_sp, n_tp, rows, chans, members, width, group_chans * n_tp)
-        ),
-        out_shape=jax.ShapeDtypeStruct((rows, model), bf16),
-        in_specs=[vmem] * 3,
-        out_specs=vmem,
-        scratch_shapes=[
-            pltpu.VMEM((n_sp, 2 * chans + 16, total // 2), bf16),
-            pltpu.VMEM((n_tp + 1, 8, total // 2), f32),
-            pltpu.VMEM((n_tp, n_sp // 2, rows, 2 * cols), bf16),
-            pltpu.VMEM((n_tp, n_sp // 2, rows, 2 * cols), bf16),
-            pltpu.VMEM((n_sp // 2, rows, 2 * cols), bf16),
-            dma((n_z,)),
-            dma((n_z,)),
-            dma((n_z,)),
-            dma((n_z,)),
-            dma((n_tp,)),
-            dma((n_tp,)),
-            dma((n_tp, n_sp // 2)),
-            dma((n_tp, n_sp // 2)),
-            dma((n_sp // 2, 2)),
-            dma((n_sp // 2, 2)),
-        ],
-        compiler_params=pltpu.CompilerParams(collective_id=1, has_side_effects=True),
-        name="output",
-    )(sent, weights_out, params)
 
 
 def layer(n_sp, n_tp, *arrays):

time: 89.4 us -> 73 us (0.82)
  Pallas kernels: 84.3 us -> 71.2 us
  local copies, waits for them, and re-layouts: 4.54 us -> 1.57 us
    pallas_call x3 -> x1, Pallas kernels: 84.3 us -> 71.2 us  [spread_channels(): pl.pallas_call(functools.partial(layer_kernel, (n_sp, n_tp, rows, depth,...]
    concatenate x2 -> x0, local copies, waits for them, and re-layouts: 1.57 us -> none  [spread_channels(): jnp.concatenate([depthwise_filter_taps.T, head_norm_gain[:, None], forget...]
    unnamed x11 -> x1, local copies, waits for them, and re-layouts: 2.37 us -> 1.57 us
where the time goes in v4:
time: 73 us; the launch traced here: 72.7 us
  Pallas kernels  71.2 us (98%)
  local copies, waits for them, and re-layouts  1.57 us (2%)
    pallas_call x1, Pallas kernels, spread_channels(): pl.pallas_call(functools.partial(layer_kernel, (n_sp, n_tp, rows, depth,...  71.2 us
    unnamed x1, local copies, waits for them, and re-layouts  1.57 us

profile of v4, /device:TPU:0, one launch (start us, length us, event | category | flops | bytes accessed | tf_op | source)
XLA Modules:
  0.0 72.7 jit_solution(18347634165143211455)
XLA Ops:
  0.0 71.2 %layer.1 = bf16[32,2048]{1,0:T(8,128)(2,1)} custom-call(bf16[32,2048]{1,0:T(8,128)(2,1)} %x_hbm.1, f32[1,2048]{1,0:T(1,128)} %bitcast.5, f32[2,128]{1,0:T(2,128)} %j_ref.1, f32[31,256]{1,0:T(8,128)} %taps.1, f32[1,256]{1,0:T(1,128)} %bitcast.6, f32[1,256]{1,0:T(1,128)} %bitcast.7, f32[1,256]{1,0:T(1,128)} %bitcast.8, f32[1,256]{1,0:T(1,128)} %bitcast.9, ...), custom_call_target="tpu_custom_call" | custom-call | tf_op jit(solution)/shard_map/layer/pallas_call | solution.py:687
  71.2 1.6 %copy.18 = bf16[32,2048]{1,0:T(8,128)(2,1)} copy(bf16[32,2048]{1,0:T(8,128)(2,1)} %layer.1) | data formatting | bytes 262144

commit v5 on v4

--- a/solution.py
+++ b/solution.py
@@ -324,7 +324,10 @@
         if not dy:
             if not dx:
                 launch(remote(here, here, send_x.at[dz], lane.at[number(0, 1, dz)], x_peer))
-            launch(remote(here, here, send_y.at[at_number], lane.at[number(1, dx, dz)], y_peer))
+            if not (dx and dz == n_z - 1):
+                launch(remote(here, here, send_y.at[at_number], lane.at[number(1, dx, dz)], y_peer))
+        elif not dx and dz == n_z - 1:
+            launch(remote(here, here, send_y.at[at_number], lane.at[number(1, 1, dz)], x_peer))
         launch(remote(here, here, send_c.at[at_number], sib.at[at_number], c_peer))
 
     near_first = sorted(range(1, n_z), key=lambda k: min(k, n_z - k))
@@ -523,9 +526,11 @@
                 window(home, p)[...] = piece[...]
 
     sequence = list(range(1, blocks)) + [0]
-    for r in sequence:
+    for i, r in enumerate(sequence):
         project_block(r)
-    for r in sequence:
+        if i >= 2:
+            finish_block(sequence[i - 2])
+    for r in sequence[-2:]:
         finish_block(r)
     for r in range(1, blocks):
         for p in range(2):

time: 73 us -> 73 us (level)
  no operation moved by 1% of the time
where the time goes in v5:
time: 73 us; the launch traced here: 72.7 us
  Pallas kernels  71.2 us (98%)
  local copies, waits for them, and re-layouts  1.57 us (2%)
    pallas_call x1, Pallas kernels, spread_channels(): pl.pallas_call(functools.partial(layer_kernel, (n_sp, n_tp, rows, depth,...  71.2 us
    unnamed x1, local copies, waits for them, and re-layouts  1.57 us

profile of v5, /device:TPU:0, one launch (start us, length us, event | category | flops | bytes accessed | tf_op | source)
XLA Modules:
  0.0 72.7 jit_solution(7473648077275989097)
XLA Ops:
  0.0 71.2 %layer.1 = bf16[32,2048]{1,0:T(8,128)(2,1)} custom-call(bf16[32,2048]{1,0:T(8,128)(2,1)} %x_hbm.1, f32[1,2048]{1,0:T(1,128)} %bitcast.5, f32[2,128]{1,0:T(2,128)} %j_ref.1, f32[31,256]{1,0:T(8,128)} %taps.1, f32[1,256]{1,0:T(1,128)} %bitcast.6, f32[1,256]{1,0:T(1,128)} %bitcast.7, f32[1,256]{1,0:T(1,128)} %bitcast.8, f32[1,256]{1,0:T(1,128)} %bitcast.9, ...), custom_call_target="tpu_custom_call" | custom-call | tf_op jit(solution)/shard_map/layer/pallas_call | solution.py:692
  71.2 1.6 %copy.18 = bf16[32,2048]{1,0:T(8,128)(2,1)} copy(bf16[32,2048]{1,0:T(8,128)(2,1)} %layer.1) | data formatting | bytes 262144
